TPU v7x, 256 devices: a whole 4x4x8 slice. The times are simulated.
256 devices in a mesh: ra: 32 (over z, y), cb: 4 (over x), dp: 2 (over core).
Axes of the slice: x: 4, y: 4, z: 8, core: 2. Of those that a mesh axis runs over, the one named last changes fastest.
Arguments:
- stream: bfloat16 [4, 64, 4096], P('dp', None, 'ra'), may hold values from -16 to 16
- norm_gain: bfloat16 [2, 4096], P(None, 'ra'), may hold values from 0.099609375 to 1.8984375
- gate_weight: bfloat16 [2, 4096, 12288], P(None, 'ra', 'cb'), may hold values from -0.09375 to 0.09375
- value_weight: bfloat16 [2, 4096, 12288], P(None, 'ra', 'cb'), may hold values from -0.09375 to 0.09375
- gate_taps: bfloat16 [2, 3, 12288], P(None, None, 'cb'), may hold values from -3 to 3
- value_taps: bfloat16 [2, 3, 12288], P(None, None, 'cb'), may hold values from -3 to 3
- gate_bias: bfloat16 [2, 12288], P(None, 'cb'), may hold values from -3 to 3
- value_bias: bfloat16 [2, 12288], P(None, 'cb'), may hold values from -3 to 3
- down_weight: bfloat16 [2, 12288, 4096], P(None, 'cb', 'ra'), may hold values from -0.0546875 to 0.0546875
- final_gain: bfloat16 [4096], P('ra'), may hold values from 0.099609375 to 1.8984375
Outputs:
- mixed: bfloat16 [4, 64, 4096], P('dp', None, 'ra')
All inputs are finite; a program needn't handle non-finite values.
Results may differ from a plain program's by a relative error of at most 0.035.
Values may be sent and summed in bfloat16 or wider, within the bound.
No kernel may reach another device: no remote copies, remote signals or barrier semaphores. Data moves between devices by JAX's collectives and lax.ppermute only.
A program may use at most 64 MiB of HBM per device.

v0:
```python
import jax
import jax.numpy as jnp
from jax import lax
from jax.sharding import Mesh
from jax.sharding import PartitionSpec as P

D = 4096
LAYERS = 2
RA = ("ra_0", "ra_1")


EPS = 1e-06


def sent_to_all(x, axis):
    copies = jnp.broadcast_to(x, (lax.axis_size(axis), *x.shape))
    return lax.all_to_all(copies, axis, split_axis=0, concat_axis=0, tiled=True)


def of_everyone(x, axis):
    return sent_to_all(x, axis).sum(axis=0)


def cut_along(x, dim, size):
    dims = x.shape
    parts = x.reshape(*dims[:dim], size, dims[dim] // size, *dims[dim + 1 :])
    return jnp.moveaxis(parts, dim, 0)


def summed_on_arrival(x, axis, dim):
    parts = cut_along(x, dim, lax.axis_size(axis))
    arrived = lax.all_to_all(parts, axis, split_axis=0, concat_axis=0, tiled=True)
    return arrived.astype(jnp.float32).sum(axis=0)


def side_by_side(arrays, axis, dim, along):
    ends, at = ([], 0)
    for a in arrays[:-1]:
        at += a.shape[along]
        ends.append(at)
    both = jnp.concatenate(arrays, axis=along)
    return tuple(jnp.split(summed_on_arrival(both, axis, dim), ends, axis=along))


def whole_of(x, axes, dim):
    if not axes:
        return x
    nearer = lax.all_gather(x, axes[-1], axis=dim, tiled=True)
    return whole_of(nearer, axes[:-1], dim)


def of_everyone_2(x, axis):
    return sent_to_all(x, axis).astype(jnp.float32).sum(axis=0)


def rms_scaled(stream_in, gain_row):
    values = stream_in.astype(jnp.float32)
    squares = of_everyone(jnp.sum(values * values, axis=-1, keepdims=True), RA)
    return values * lax.rsqrt(squares / D + EPS) * gain_row.astype(jnp.float32)


def causal_mix(up_rows, taps, bias):
    length = up_rows.shape[1]
    count = taps.shape[0]
    padded = jnp.pad(up_rows.astype(jnp.float32), ((0, 0), (count - 1, 0), (0, 0)))
    result = jnp.zeros(up_rows.shape, jnp.float32) + bias.astype(jnp.float32)
    for tap_index in range(count):
        result = result + padded[:, tap_index : tap_index + length] * taps[tap_index].astype(
            jnp.float32
        )
    return result


def body(
    stream,
    norm_gain,
    gate_weight,
    value_weight,
    gate_taps,
    value_taps,
    gate_bias,
    value_bias,
    down_weight,
    final_gain,
):
    batch_rows, length, width = stream.shape
    ff_local = gate_weight.shape[2]
    current = stream
    for layer_index in range(LAYERS):
        normed = rms_scaled(current, norm_gain[layer_index]).astype(jnp.bfloat16).reshape(-1, width)
        gate_partial = jnp.dot(
            normed, gate_weight[layer_index], preferred_element_type=jnp.float32
        ).reshape(batch_rows, length, ff_local)
        value_partial = jnp.dot(
            normed, value_weight[layer_index], preferred_element_type=jnp.float32
        ).reshape(batch_rows, length, ff_local)
        down_local = down_weight[layer_index]
        gate_sum, value_sum = side_by_side(
            (gate_partial.astype(jnp.bfloat16), value_partial.astype(jnp.bfloat16)), RA, 2, 0
        )
        slice_width = gate_sum.shape[2]
        lower = lax.axis_index(RA) * slice_width
        gate_slice = lax.dynamic_slice_in_dim(gate_taps[layer_index], lower, slice_width, 1)
        value_slice = lax.dynamic_slice_in_dim(value_taps[layer_index], lower, slice_width, 1)
        gate_shift = lax.dynamic_slice_in_dim(gate_bias[layer_index], lower, slice_width, 0)
        value_shift = lax.dynamic_slice_in_dim(value_bias[layer_index], lower, slice_width, 0)
        gate_conv = causal_mix(gate_sum.astype(jnp.bfloat16), gate_slice, gate_shift)
        value_conv = causal_mix(value_sum.astype(jnp.bfloat16), value_slice, value_shift)
        hidden = (jax.nn.gelu(gate_conv) * value_conv).astype(jnp.bfloat16)
        block_rows = whole_of(hidden, RA, 2)
        count = block_rows.shape[2]
        term = jnp.dot(
            block_rows.reshape(-1, count), down_local, preferred_element_type=jnp.float32
        )
        branch = of_everyone_2(term.astype(jnp.bfloat16), "cb").astype(jnp.float32)
        current = (
            0.5 * current.astype(jnp.float32) + branch.reshape(batch_rows, length, width)
        ).astype(jnp.bfloat16)
    return rms_scaled(current, final_gain).astype(jnp.bfloat16)


def solution(mesh):
    split = Mesh(
        mesh.devices.reshape(8, 4, mesh.shape["cb"], mesh.shape["dp"]), ("ra_0", "ra_1", "cb", "dp")
    )
    return jax.shard_map(
        body,
        mesh=split,
        in_specs=(
            P("dp", None, RA),
            P(None, RA),
            P(None, RA, "cb"),
            P(None, RA, "cb"),
            P(None, None, "cb"),
            P(None, None, "cb"),
            P(None, "cb"),
            P(None, "cb"),
            P(None, "cb", RA),
            P(RA),
        ),
        out_specs=P("dp", None, RA),
        check_vma=False,
    )
```

profile of v0, /device:TPU:2, one launch (start us, length us, event | category | flops | bytes accessed | tf_op | source)
XLA Modules:
  0.0 268.5 jit_solution(10192891672005312421)
XLA Ops:
  0.0 1.0 fusion.41
  1.0 0.7 reshape.162
  1.7 11.5 %all-to-all-start = ((f32[32,1,128]{2,1,0:T(1,128)}), f32[32,1,128]{2,1,0:T(1,128)S(1)}, u32[]{:S(2)}, u32[]{:S(2)}) async-start(f32[32,1,128]{2,1,0:T(1,128)} %reshape.162), calls=%async_computation | async-start | bytes 32768 | tf_op jit(solution)/shard_map/all_to_all | solution.py:17
  13.2 0.7 bitcast_convert_fusion
  13.9 8.9 %all-to-all-done = f32[32,1,128]{2,1,0:T(1,128)S(1)} async-done(((f32[32,1,128]{2,1,0:T(1,128)}), f32[32,1,128]{2,1,0:T(1,128)S(1)}, u32[]{:S(2)}, u32[]{:S(2)}) %all-to-all-start) | async-done | bytes 16416 | tf_op jit(solution)/shard_map/all_to_all | solution.py:17
  22.9 0.5 broadcast.94
  23.4 0.7 reduce.5
  24.2 1.6 convolution_convert_fusion.2
  25.8 0.4 convolution_convert_fusion.3
  26.2 1.3 pad_maximum_fusion
  27.5 3.6 %reshape.134 = bf16[4,64,32,96]{3,2,1,0:T(8,128)(2,1)S(1)} reshape(bf16[4,64,3072]{2,1,0:T(8,128)(2,1)} %pad_maximum_fusion) | data formatting | bytes 3145728 | tf_op jit(solution)/shard_map/reshape | solution.py:26
  31.1 2.2 copy.32
  33.3 4.2 %all-to-all-start.1 = ((bf16[32,4,64,96]{3,2,1,0:T(8,128)(2,1)}), bf16[32,4,64,96]{3,2,1,0:T(8,128)(2,1)S(1)}, u32[]{:S(2)}, u32[]{:S(2)}) async-start(bf16[32,4,64,96]{3,2,1,0:T(8,128)(2,1)} %bitcast.133), calls=%async_computation.1 | async-start | bytes 4194304 | tf_op jit(solution)/shard_map/all_to_all | solution.py:32
  37.7 0.1 fusion.84
  37.8 49.3 %all-to-all-done.1 = bf16[32,4,64,96]{3,2,1,0:T(8,128)(2,1)S(1)} async-done(((bf16[32,4,64,96]{3,2,1,0:T(8,128)(2,1)}), bf16[32,4,64,96]{3,2,1,0:T(8,128)(2,1)S(1)}, u32[]{:S(2)}, u32[]{:S(2)}) %all-to-all-start.1) | async-done | bytes 1572896 | tf_op jit(solution)/shard_map/all_to_all | solution.py:32
  87.1 0.4 reduce.3
  87.6 0.1 fusion.22
  87.7 0.1 copy.24
  87.8 12.2 %all_gather.12 = bf16[2,64,384]{1,0,2:T(2,128)(2,1)S(1)} all-gather(bf16[2,64,96]{1,0,2:T(2,128)(2,1)S(1)} %copy.24), channel_id=1, replica_groups=mesh['ra_0'=8,'ra_1'=4,'cb'=4,'dp'=2] {'ra_1'}, dimensions={2}, use_global_device_ids=true | all-gather | bytes 122880 | tf_op jit(solution)/shard_map/all_gather | solution.py:48
  100.0 0.1 copy.25
  100.1 26.6 %all_gather.13 = bf16[2,64,3072]{2,1,0:T(8,128)(2,1)S(1)} all-gather(bf16[2,64,384]{2,1,0:T(8,128)(2,1)S(1)} %copy.25), channel_id=1, replica_groups=mesh['ra_0'=8,'ra_1'=4,'cb'=4,'dp'=2] {'ra_0'}, dimensions={2}, use_global_device_ids=true | all-gather | bytes 884736 | tf_op jit(solution)/shard_map/all_gather | solution.py:48
  126.7 1.5 convolution_convert_fusion.5
  128.3 9.3 %all_to_all.35 = bf16[4,128,128]{2,1,0:T(8,128)(2,1)S(1)} all-to-all(bf16[4,128,128]{2,1,0:T(8,128)(2,1)S(1)} %broadcast_in_dim.11), channel_id=1, replica_groups=mesh['ra_0'=8,'ra_1'=4,'cb'=4,'dp'=2] {'cb'}, dimensions={0} | all-to-all | bytes 262144 | tf_op jit(solution)/shard_map/all_to_all | solution.py:17
  137.6 0.1 fusion.53
  137.7 0.1 reshape.164
  137.8 15.4 %all_to_all.36 = f32[32,1,128]{2,1,0:T(1,128)S(1)} all-to-all(f32[32,1,128]{2,1,0:T(1,128)S(1)} %reshape.164), channel_id=1, replica_groups=mesh['ra_0'=8,'ra_1'=4,'cb'=4,'dp'=2] {'ra_0','ra_1'}, dimensions={0} | all-to-all | bytes 32768 | tf_op jit(solution)/shard_map/all_to_all | solution.py:17
  153.3 0.7 reduce.6
  154.1 0.4 convolution_convert_fusion
  154.5 0.4 convolution_convert_fusion.1
  154.9 1.3 pad_maximum_fusion.1
  156.2 3.6 %reshape.137 = bf16[4,64,32,96]{3,2,1,0:T(8,128)(2,1)S(1)} reshape(bf16[4,64,3072]{2,1,0:T(8,128)(2,1)} %pad_maximum_fusion.1) | data formatting | bytes 3145728 | tf_op jit(solution)/shard_map/reshape | solution.py:26
  159.8 2.2 copy.31
  162.0 4.0 %all-to-all-start.4 = ((bf16[32,4,64,96]{3,2,1,0:T(8,128)(2,1)}), bf16[32,4,64,96]{3,2,1,0:T(8,128)(2,1)S(1)}, u32[]{:S(2)}, u32[]{:S(2)}) async-start(bf16[32,4,64,96]{3,2,1,0:T(8,128)(2,1)} %bitcast.134), calls=%async_computation.4 | async-start | bytes 4194304 | tf_op jit(solution)/shard_map/all_to_all | solution.py:32
  166.1 36.5 %all-to-all-done.4 = bf16[32,4,64,96]{3,2,1,0:T(8,128)(2,1)S(1)} async-done(((bf16[32,4,64,96]{3,2,1,0:T(8,128)(2,1)}), bf16[32,4,64,96]{3,2,1,0:T(8,128)(2,1)S(1)}, u32[]{:S(2)}, u32[]{:S(2)}) %all-to-all-start.4) | async-done | bytes 1572896 | tf_op jit(solution)/shard_map/all_to_all | solution.py:32
  202.6 0.4 reduce.4
  203.1 0.1 fusion.34
  203.2 0.1 copy.27
  203.3 12.7 %all_gather.14 = bf16[2,64,384]{1,0,2:T(2,128)(2,1)S(1)} all-gather(bf16[2,64,96]{1,0,2:T(2,128)(2,1)S(1)} %copy.27), channel_id=1, replica_groups=mesh['ra_0'=8,'ra_1'=4,'cb'=4,'dp'=2] {'ra_1'}, dimensions={2}, use_global_device_ids=true | all-gather | bytes 122880 | tf_op jit(solution)/shard_map/all_gather | solution.py:48
  216.0 0.1 copy.28
  216.2 25.9 %all_gather.15 = bf16[2,64,3072]{2,1,0:T(8,128)(2,1)S(1)} all-gather(bf16[2,64,384]{2,1,0:T(8,128)(2,1)S(1)} %copy.28), channel_id=1, replica_groups=mesh['ra_0'=8,'ra_1'=4,'cb'=4,'dp'=2] {'ra_0'}, dimensions={2}, use_global_device_ids=true | all-gather | bytes 884736 | tf_op jit(solution)/shard_map/all_gather | solution.py:48
  242.0 0.4 convolution_convert_fusion.4
  242.4 8.1 %all_to_all.37 = bf16[4,128,128]{2,1,0:T(8,128)(2,1)S(1)} all-to-all(bf16[4,128,128]{2,1,0:T(8,128)(2,1)S(1)} %broadcast_in_dim.13), channel_id=1, replica_groups=mesh['ra_0'=8,'ra_1'=4,'cb'=4,'dp'=2] {'cb'}, dimensions={0} | all-to-all | bytes 262144 | tf_op jit(solution)/shard_map/all_to_all | solution.py:17
  250.5 0.1 fusion.36
  250.7 0.7 reshape.166
  251.4 6.0 %all-to-all-start.6 = ((f32[32,1,128]{2,1,0:T(1,128)}), f32[32,1,128]{2,1,0:T(1,128)S(1)}, u32[]{:S(2)}, u32[]{:S(2)}) async-start(f32[32,1,128]{2,1,0:T(1,128)} %reshape.166), calls=%async_computation.6 | async-start | bytes 32768 | tf_op jit(solution)/shard_map/all_to_all | solution.py:17
  257.3 9.7 %all-to-all-done.6 = f32[32,1,128]{2,1,0:T(1,128)S(1)} async-done(((f32[32,1,128]{2,1,0:T(1,128)}), f32[32,1,128]{2,1,0:T(1,128)S(1)}, u32[]{:S(2)}, u32[]{:S(2)}) %all-to-all-start.6) | async-done | bytes 16416 | tf_op jit(solution)/shard_map/all_to_all | solution.py:17
  267.0 0.7 reduce.7
  267.8 0.7 fusion.38
  (46 shorter events, 1.0 us)
Async XLA Ops:
  0.0 25.8 %copy-start.3 = (bf16[2,64,128]{2,1,0:T(8,128)(2,1)S(1)}, bf16[2,64,128]{2,1,0:T(8,128)(2,1)}, u32[]{:S(2)}) copy-start(bf16[2,64,128]{2,1,0:T(8,128)(2,1)} %param.10) | copy-start | bytes 98308
  0.0 25.8 %copy-start.1 = (bf16[2,128,3072]{2,1,0:T(8,128)(2,1)S(1)}, bf16[2,128,3072]{2,1,0:T(8,128)(2,1)}, u32[]{:S(2)}) copy-start(bf16[2,128,3072]{2,1,0:T(8,128)(2,1)} %param.12) | copy-start | bytes 4718596
  1.7 21.2 %all-to-all-start = ((f32[32,1,128]{2,1,0:T(1,128)}), f32[32,1,128]{2,1,0:T(1,128)S(1)}, u32[]{:S(2)}, u32[]{:S(2)}) async-start(f32[32,1,128]{2,1,0:T(1,128)} %reshape.162), calls=%async_computation | async-start | bytes 32768 | tf_op jit(solution)/shard_map/all_to_all | solution.py:17
  33.3 4.2 %copy-start.6 = (bf16[2,3072]{1,0:T(2,128)(2,1)S(1)}, bf16[2,3072]{1,0:T(2,128)(2,1)}, u32[]{:S(2)}) copy-start(bf16[2,3072]{1,0:T(2,128)(2,1)} %param.16) | copy-start | bytes 36868
  33.3 4.2 %copy-start.7 = (bf16[2,3072]{1,0:T(2,128)(2,1)S(1)}, bf16[2,3072]{1,0:T(2,128)(2,1)}, u32[]{:S(2)}) copy-start(bf16[2,3072]{1,0:T(2,128)(2,1)} %param.17) | copy-start | bytes 36868
  33.3 4.3 %copy-start.4 = (bf16[2,3,3072]{2,0,1:T(2,128)(2,1)S(1)}, bf16[2,3,3072]{2,0,1:T(2,128)(2,1)}, u32[]{:S(2)}) copy-start(bf16[2,3,3072]{2,0,1:T(2,128)(2,1)} %param.14) | copy-start | bytes 110596
  33.3 4.4 %copy-start.5 = (bf16[2,3,3072]{2,0,1:T(2,128)(2,1)S(1)}, bf16[2,3,3072]{2,0,1:T(2,128)(2,1)}, u32[]{:S(2)}) copy-start(bf16[2,3,3072]{2,0,1:T(2,128)(2,1)} %param.15) | copy-start | bytes 110596
  33.3 53.9 %all-to-all-start.1 = ((bf16[32,4,64,96]{3,2,1,0:T(8,128)(2,1)}), bf16[32,4,64,96]{3,2,1,0:T(8,128)(2,1)S(1)}, u32[]{:S(2)}, u32[]{:S(2)}) async-start(bf16[32,4,64,96]{3,2,1,0:T(8,128)(2,1)} %bitcast.133), calls=%async_computation.1 | async-start | bytes 4194304 | tf_op jit(solution)/shard_map/all_to_all | solution.py:32
  100.1 53.9 %copy-start = (bf16[2,128,3072]{2,1,0:T(8,128)(2,1)S(1)}, bf16[2,128,3072]{2,1,0:T(8,128)(2,1)}, u32[]{:S(2)}) copy-start(bf16[2,128,3072]{2,1,0:T(8,128)(2,1)} %param.13) | copy-start | bytes 4718596
  128.2 26.3 %copy-start.2 = (bf16[2,128,3072]{2,1,0:T(8,128)(2,1)S(1)}, bf16[2,128,3072]{2,1,0:T(8,128)(2,1)}, u32[]{:S(2)}) copy-start(bf16[2,128,3072]{2,1,0:T(8,128)(2,1)} %param.12) | copy-start | bytes 4718596
  162.0 40.6 %all-to-all-start.4 = ((bf16[32,4,64,96]{3,2,1,0:T(8,128)(2,1)}), bf16[32,4,64,96]{3,2,1,0:T(8,128)(2,1)S(1)}, u32[]{:S(2)}, u32[]{:S(2)}) async-start(bf16[32,4,64,96]{3,2,1,0:T(8,128)(2,1)} %bitcast.134), calls=%async_computation.4 | async-start | bytes 4194304 | tf_op jit(solution)/shard_map/all_to_all | solution.py:32
  203.0 39.0 %copy-start.8 = (bf16[2,3072,128]{2,1,0:T(8,128)(2,1)S(1)}, bf16[2,3072,128]{2,1,0:T(8,128)(2,1)}, u32[]{:S(2)}) copy-start(bf16[2,3072,128]{2,1,0:T(8,128)(2,1)} %param.18) | copy-start | bytes 4718596
  216.2 41.2 %copy-start.9 = (bf16[128]{0:T(256)(128)(2,1)S(1)}, bf16[128]{0:T(256)(128)(2,1)}, u32[]{:S(2)}) copy-start(bf16[128]{0:T(256)(128)(2,1)} %param.19) | copy-start | bytes 772
  251.4 15.6 %all-to-all-start.6 = ((f32[32,1,128]{2,1,0:T(1,128)}), f32[32,1,128]{2,1,0:T(1,128)S(1)}, u32[]{:S(2)}, u32[]{:S(2)}) async-start(f32[32,1,128]{2,1,0:T(1,128)} %reshape.166), calls=%async_computation.6 | async-start | bytes 32768 | tf_op jit(solution)/shard_map/all_to_all | solution.py:17
where the time goes:
time: 269 us
  blocking collectives  110 us (41%)
  waiting for transfers between devices  104 us (39%)
  starting transfers between devices  25.6 us (10%)
  local copies, waits for them, and re-layouts  14.6 us (5%)
  other arithmetic  8.74 us (3%)
  matrix products  4.65 us (2%)
    all_to_all x2, waiting for transfers between devices, summed_on_arrival(): lax.all_to_all(parts, axis, split_axis=0, concat_axis=0, tiled=True)  85.8 us
    all_gather x4, blocking collectives, whole_of(): nearer = lax.all_gather(x, axes[-1], axis=dim, tiled=True)  77.4 us
    all_to_all x3, blocking collectives, sent_to_all(): return lax.all_to_all(copies, axis, split_axis=0, concat_axis=0, tiled=True)  32.8 us
    all_to_all x2, waiting for transfers between devices, sent_to_all(): return lax.all_to_all(copies, axis, split_axis=0, concat_axis=0, tiled=True)  18.6 us
    all_to_all x2, starting transfers between devices, sent_to_all(): return lax.all_to_all(copies, axis, split_axis=0, concat_axis=0, tiled=True)  17.4 us
    reshape x4, local copies, waits for them, and re-layouts, cut_along(): parts = x.reshape(*dims[:dim], size, dims[dim] // size, *dims[dim + 1:])  11.5 us
    all_to_all x2, starting transfers between devices, summed_on_arrival(): lax.all_to_all(parts, axis, split_axis=0, concat_axis=0, tiled=True)  8.16 us
  transfers between devices with their start and end apart: 4, of which 4 were waited for; matrix products, arithmetic and copies ran while one was open for 0% of the time, Pallas kernels for 0%

commit v1 on v0

v1 whole, which is shorter than its diff:
```python
import jax
import jax.numpy as jnp
from jax import lax
from jax.sharding import Mesh
from jax.sharding import PartitionSpec as P

D = 4096
LAYERS = 2
RA = ("ra_0", "ra_1")
EPS = 1e-06
F32 = jnp.float32
BF16 = jnp.bfloat16
TN = (((0,), (0,)), ((), ()))


def exchanged(x, axis):
    return lax.all_to_all(x, axis, split_axis=0, concat_axis=0, tiled=True)


def to_everyone(x, axis):
    copies = jnp.broadcast_to(x[None], (lax.axis_size(axis), *x.shape))
    return exchanged(copies, axis)


def two_halves(row):
    high = row.astype(BF16)
    low = (row - high.astype(F32)).astype(BF16)
    return jnp.concatenate([high, low], axis=0)


def shifted(x, by, position):
    moved = jnp.pad(x, ((0, 0), (by, 0)))[:, : x.shape[1]]
    return jnp.where(position >= by, moved, 0.0)


def causal_mix(rows, columns, position):
    x = rows.astype(F32)
    return (
        columns[:, 3:4]
        + shifted(x, 2, position) * columns[:, 0:1]
        + shifted(x, 1, position) * columns[:, 1:2]
        + x * columns[:, 2:3]
    )


def body(
    stream,
    norm_gain,
    gate_weight,
    value_weight,
    gate_taps,
    value_taps,
    gate_bias,
    value_bias,
    down_weight,
    final_gain,
):
    batch_rows, length, width = stream.shape
    tokens = batch_rows * length
    members = lax.axis_size(RA)
    units = gate_weight.shape[2] // members
    position = lax.broadcasted_iota(jnp.int32, (1, tokens), 1) % length
    lower = lax.axis_index(RA) * units
    table = jnp.concatenate(
        [gate_taps, gate_bias[:, None], value_taps, value_bias[:, None]], axis=1
    )
    table = lax.dynamic_slice_in_dim(table, lower, units, 2)
    table = jnp.swapaxes(table, 1, 2).astype(F32)
    gains = norm_gain.astype(F32)[:, :, None]
    current = stream.reshape(tokens, width).T
    for layer in range(LAYERS):
        values = current.astype(F32)
        squares = jnp.sum(values * values, axis=0, keepdims=True)
        gained = (values * gains[layer]).astype(BF16)
        gate = lax.dot_general(gate_weight[layer], gained, TN, preferred_element_type=F32)
        value = lax.dot_general(value_weight[layer], gained, TN, preferred_element_type=F32)
        parts = jnp.concatenate(
            [
                gate.astype(BF16).reshape(members, units, tokens),
                value.astype(BF16).reshape(members, units, tokens),
                jnp.broadcast_to(two_halves(squares)[None], (members, 2, tokens)),
            ],
            axis=1,
        )
        total = exchanged(parts, RA).astype(F32).sum(axis=0)
        scale = lax.rsqrt((total[2 * units] + total[2 * units + 1])[None] / D + EPS)
        gate_up = (total[:units] * scale).astype(BF16)
        value_up = (total[units : 2 * units] * scale).astype(BF16)
        gate_conv = causal_mix(gate_up, table[layer, :, 0:4], position)
        value_conv = causal_mix(value_up, table[layer, :, 4:8], position)
        hidden = (jax.nn.gelu(gate_conv) * value_conv).astype(BF16)
        block = to_everyone(hidden, RA).reshape(-1, tokens)
        term = lax.dot_general(down_weight[layer], block, TN, preferred_element_type=F32)
        branch = to_everyone(term.astype(BF16), "cb").astype(F32).sum(axis=0)
        current = (0.5 * values + branch).astype(BF16)
    values = current.astype(F32)
    squares = jnp.sum(values * values, axis=0, keepdims=True)
    total = to_everyone(two_halves(squares), RA).astype(F32).sum(axis=(0, 1))
    mixed = values * lax.rsqrt(total[None] / D + EPS) * final_gain.astype(F32)[:, None]
    return mixed.astype(BF16).T.reshape(batch_rows, length, width)


def solution(mesh):
    split = Mesh(
        mesh.devices.reshape(8, 4, mesh.shape["cb"], mesh.shape["dp"]), ("ra_0", "ra_1", "cb", "dp")
    )
    return jax.shard_map(
        body,
        mesh=split,
        in_specs=(
            P("dp", None, RA),
            P(None, RA),
            P(None, RA, "cb"),
            P(None, RA, "cb"),
            P(None, None, "cb"),
            P(None, None, "cb"),
            P(None, "cb"),
            P(None, "cb"),
            P(None, "cb", RA),
            P(RA),
        ),
        out_specs=P("dp", None, RA),
        check_vma=False,
    )
```

time: 269 us -> 197 us (0.73)
  blocking collectives: 110 us -> 61.8 us
  waiting for transfers between devices: 104 us -> 91.6 us
  local copies, waits for them, and re-layouts: 14.6 us -> 3.58 us
    all_gather x4 -> x0, blocking collectives: 77.4 us -> none  [whole_of(): nearer = lax.all_gather(x, axes[-1], axis=dim, tiled=True)]
    all_to_all x3, blocking collectives: 32.8 us -> 61.8 us  [exchanged(): return lax.all_to_all(x, axis, split_axis=0, concat_axis=0, tiled=True)]
    all_to_all x4, waiting for transfers between devices: 104 us -> 91.6 us  [exchanged(): return lax.all_to_all(x, axis, split_axis=0, concat_axis=0, tiled=True)]
    reshape x4 -> x0, local copies, waits for them, and re-layouts: 11.5 us -> none  [cut_along(): parts = x.reshape(*dims[:dim], size, dims[dim] // size, *dims[dim + 1:])]
where the time goes in v1:
time: 197 us; the launch traced here: 196 us
  waiting for transfers between devices  91.6 us (46%)
  blocking collectives  61.8 us (31%)
  starting transfers between devices  26.4 us (13%)
  other arithmetic  6.07 us (3%)
  matrix products  5.86 us (3%)
  local copies, waits for them, and re-layouts  3.58 us (2%)
    all_to_all x4, waiting for transfers between devices, exchanged(): return lax.all_to_all(x, axis, split_axis=0, concat_axis=0, tiled=True)  91.6 us
    all_to_all x3, blocking collectives, exchanged(): return lax.all_to_all(x, axis, split_axis=0, concat_axis=0, tiled=True)  61.8 us
    all_to_all x4, starting transfers between devices, exchanged(): return lax.all_to_all(x, axis, split_axis=0, concat_axis=0, tiled=True)  26.4 us
  transfers between devices with their start and end apart: 4, of which 4 were waited for; matrix products, arithmetic and copies ran while one was open for 0% of the time, Pallas kernels for 0%

profile of v1, /device:TPU:2, one launch (start us, length us, event | category | flops | bytes accessed | tf_op | source)
XLA Modules:
  0.0 195.8 jit_solution(13130782684340182381)
XLA Ops:
  0.0 0.7 convert_element_type.265
  0.7 0.9 fusion.24
  1.6 1.5 fusion
  3.0 0.4 copy.48
  3.4 1.5 fusion.1
  4.9 0.4 copy.49
  5.3 1.3 pad_maximum_fusion
  6.6 11.6 %all-to-all-start = ((bf16[32,194,128]{2,1,0:T(8,128)(2,1)}), bf16[32,194,128]{2,1,0:T(8,128)(2,1)S(1)}, u32[]{:S(2)}, u32[]{:S(2)}) async-start(bf16[32,194,128]{2,1,0:T(8,128)(2,1)} %pad_maximum_fusion), calls=%async_computation | async-start | bytes 3276800 | tf_op jit(solution)/shard_map/all_to_all | solution.py:17
  18.3 0.0 copy-done.2
  18.3 0.0 copy-done.3
  18.3 0.0 copy-done.4
  18.3 0.0 copy-done.5
  18.3 0.1 convert_bitcast_fusion
  18.5 40.3 %all-to-all-done = bf16[32,194,128]{2,1,0:T(8,128)(2,1)S(1)} async-done(((bf16[32,194,128]{2,1,0:T(8,128)(2,1)}), bf16[32,194,128]{2,1,0:T(8,128)(2,1)S(1)}, u32[]{:S(2)}, u32[]{:S(2)}) %all-to-all-start) | async-done | bytes 1589280 | tf_op jit(solution)/shard_map/all_to_all | solution.py:17
  58.8 0.2 convert_reduce_fusion.1
  59.0 0.0 copy-start.6
  59.0 0.2 fusion.34
  59.3 0.1 broadcast_in_dim.116
  59.4 27.4 %all_to_all.35 = bf16[32,96,128]{2,1,0:T(8,128)(2,1)S(1)} all-to-all(bf16[32,96,128]{2,1,0:T(8,128)(2,1)S(1)} %broadcast_in_dim.116), channel_id=1, replica_groups=mesh['ra_0'=8,'ra_1'=4,'cb'=4,'dp'=2] {'ra_0','ra_1'}, dimensions={0} | all-to-all | bytes 1572864 | tf_op jit(solution)/shard_map/all_to_all | solution.py:17
  86.8 0.0 copy-done.6
  86.8 0.4 fusion.4
  87.3 0.1 copy.50
  87.4 0.7 broadcast_in_dim.117
  88.0 4.8 %all-to-all-start.2 = ((bf16[4,128,128]{2,1,0:T(8,128)(2,1)}), bf16[4,128,128]{2,1,0:T(8,128)(2,1)S(1)}, u32[]{:S(2)}, u32[]{:S(2)}) async-start(bf16[4,128,128]{2,1,0:T(8,128)(2,1)} %broadcast_in_dim.117), calls=%async_computation.2 | async-start | bytes 262144 | tf_op jit(solution)/shard_map/all_to_all | solution.py:17
  92.9 0.1 copy.52
  93.0 4.4 %all-to-all-done.2 = bf16[4,128,128]{2,1,0:T(8,128)(2,1)S(1)} async-done(((bf16[4,128,128]{2,1,0:T(8,128)(2,1)}), bf16[4,128,128]{2,1,0:T(8,128)(2,1)S(1)}, u32[]{:S(2)}, u32[]{:S(2)}) %all-to-all-start.2) | async-done | bytes 131104 | tf_op jit(solution)/shard_map/all_to_all | solution.py:17
  97.4 0.0 copy-done
  97.5 0.5 fusion.2
  97.9 1.6 fusion.3
  99.5 0.4 copy.53
  99.9 0.4 copy.54
  100.3 1.3 pad_maximum_fusion.1
  101.6 5.1 %all-to-all-start.3 = ((bf16[32,194,128]{2,1,0:T(8,128)(2,1)}), bf16[32,194,128]{2,1,0:T(8,128)(2,1)S(1)}, u32[]{:S(2)}, u32[]{:S(2)}) async-start(bf16[32,194,128]{2,1,0:T(8,128)(2,1)} %pad_maximum_fusion.1), calls=%async_computation.3 | async-start | bytes 3276800 | tf_op jit(solution)/shard_map/all_to_all | solution.py:17
  106.8 37.5 %all-to-all-done.3 = bf16[32,194,128]{2,1,0:T(8,128)(2,1)S(1)} async-done(((bf16[32,194,128]{2,1,0:T(8,128)(2,1)}), bf16[32,194,128]{2,1,0:T(8,128)(2,1)S(1)}, u32[]{:S(2)}, u32[]{:S(2)}) %all-to-all-start.3) | async-done | bytes 1589280 | tf_op jit(solution)/shard_map/all_to_all | solution.py:17
  144.2 0.2 convert_reduce_fusion
  144.5 0.2 fusion.43
  144.7 0.1 broadcast_in_dim.119
  144.9 26.0 %all_to_all.36 = bf16[32,96,128]{2,1,0:T(8,128)(2,1)S(1)} all-to-all(bf16[32,96,128]{2,1,0:T(8,128)(2,1)S(1)} %broadcast_in_dim.119), channel_id=1, replica_groups=mesh['ra_0'=8,'ra_1'=4,'cb'=4,'dp'=2] {'ra_0','ra_1'}, dimensions={0} | all-to-all | bytes 1572864 | tf_op jit(solution)/shard_map/all_to_all | solution.py:17
  170.9 0.0 copy-done.7
  170.9 0.4 fusion.5
  171.3 0.1 copy.55
  171.5 8.4 %all_to_all.37 = bf16[4,128,128]{2,1,0:T(8,128)(2,1)S(1)} all-to-all(bf16[4,128,128]{2,1,0:T(8,128)(2,1)S(1)} %broadcast_in_dim.120), channel_id=1, replica_groups=mesh['ra_0'=8,'ra_1'=4,'cb'=4,'dp'=2] {'cb'}, dimensions={0} | all-to-all | bytes 262144 | tf_op jit(solution)/shard_map/all_to_all | solution.py:17
  179.9 0.6 broadcast_in_dim.121
  180.5 4.9 %all-to-all-start.6 = ((bf16[32,2,128]{2,1,0:T(2,128)(2,1)}), bf16[32,2,128]{2,1,0:T(2,128)(2,1)S(1)}, u32[]{:S(2)}, u32[]{:S(2)}) async-start(bf16[32,2,128]{2,1,0:T(2,128)(2,1)} %broadcast_in_dim.121), calls=%async_computation.6 | async-start | bytes 32768 | tf_op jit(solution)/shard_map/all_to_all | solution.py:17
  185.5 0.1 copy.51
  185.6 0.1 copy.56
  185.7 9.4 %all-to-all-done.6 = bf16[32,2,128]{2,1,0:T(2,128)(2,1)S(1)} async-done(((bf16[32,2,128]{2,1,0:T(2,128)(2,1)}), bf16[32,2,128]{2,1,0:T(2,128)(2,1)S(1)}, u32[]{:S(2)}, u32[]{:S(2)}) %all-to-all-start.6) | async-done | bytes 16416 | tf_op jit(solution)/shard_map/all_to_all | solution.py:17
  195.1 0.7 multiply_convert_fusion
  (39 shorter events, 0.4 us)
Async XLA Ops:
  6.6 11.7 %copy-start.2 = (bf16[2,3,3072]{2,0,1:T(2,128)(2,1)S(1)}, bf16[2,3,3072]{2,0,1:T(2,128)(2,1)}, u32[]{:S(2)}) copy-start(bf16[2,3,3072]{2,0,1:T(2,128)(2,1)} %param.15) | copy-start | bytes 110596
  6.6 11.7 %copy-start.3 = (bf16[2,3,3072]{2,0,1:T(2,128)(2,1)S(1)}, bf16[2,3,3072]{2,0,1:T(2,128)(2,1)}, u32[]{:S(2)}) copy-start(bf16[2,3,3072]{2,0,1:T(2,128)(2,1)} %param.14) | copy-start | bytes 110596
  6.6 11.7 %copy-start.4 = (bf16[2,3072]{1,0:T(2,128)(2,1)S(1)}, bf16[2,3072]{1,0:T(2,128)(2,1)}, u32[]{:S(2)}) copy-start(bf16[2,3072]{1,0:T(2,128)(2,1)} %param.17) | copy-start | bytes 36868
  6.6 11.7 %copy-start.5 = (bf16[2,3072]{1,0:T(2,128)(2,1)S(1)}, bf16[2,3072]{1,0:T(2,128)(2,1)}, u32[]{:S(2)}) copy-start(bf16[2,3072]{1,0:T(2,128)(2,1)} %param.16) | copy-start | bytes 36868
  6.6 52.1 %all-to-all-start = ((bf16[32,194,128]{2,1,0:T(8,128)(2,1)}), bf16[32,194,128]{2,1,0:T(8,128)(2,1)S(1)}, u32[]{:S(2)}, u32[]{:S(2)}) async-start(bf16[32,194,128]{2,1,0:T(8,128)(2,1)} %pad_maximum_fusion), calls=%async_computation | async-start | bytes 3276800 | tf_op jit(solution)/shard_map/all_to_all | solution.py:17
  59.0 27.8 %copy-start.6 = (bf16[2,3072,128]{2,1,0:T(8,128)(2,1)S(1)}, bf16[2,3072,128]{2,1,0:T(8,128)(2,1)}, u32[]{:S(2)}) copy-start(bf16[2,3072,128]{2,1,0:T(8,128)(2,1)} %param.18) | copy-start | bytes 4718596
  86.8 10.6 %copy-start = (bf16[2,128,3072]{2,1,0:T(8,128)(2,1)S(1)}, bf16[2,128,3072]{2,1,0:T(8,128)(2,1)}, u32[]{:S(2)}) copy-start(bf16[2,128,3072]{2,1,0:T(8,128)(2,1)} %param.12) | copy-start | bytes 4718596
  88.0 9.3 %all-to-all-start.2 = ((bf16[4,128,128]{2,1,0:T(8,128)(2,1)}), bf16[4,128,128]{2,1,0:T(8,128)(2,1)S(1)}, u32[]{:S(2)}, u32[]{:S(2)}) async-start(bf16[4,128,128]{2,1,0:T(8,128)(2,1)} %broadcast_in_dim.117), calls=%async_computation.2 | async-start | bytes 262144 | tf_op jit(solution)/shard_map/all_to_all | solution.py:17
  101.6 42.6 %all-to-all-start.3 = ((bf16[32,194,128]{2,1,0:T(8,128)(2,1)}), bf16[32,194,128]{2,1,0:T(8,128)(2,1)S(1)}, u32[]{:S(2)}, u32[]{:S(2)}) async-start(bf16[32,194,128]{2,1,0:T(8,128)(2,1)} %pad_maximum_fusion.1), calls=%async_computation.3 | async-start | bytes 3276800 | tf_op jit(solution)/shard_map/all_to_all | solution.py:17
  144.5 26.4 %copy-start.7 = (bf16[2,3072,128]{2,1,0:T(8,128)(2,1)S(1)}, bf16[2,3072,128]{2,1,0:T(8,128)(2,1)}, u32[]{:S(2)}) copy-start(bf16[2,3072,128]{2,1,0:T(8,128)(2,1)} %param.18) | copy-start | bytes 4718596
  170.9 14.5 %copy-start.1 = (bf16[2,64,128]{2,1,0:T(8,128)(2,1)S(1)}, bf16[2,64,128]{2,1,0:T(8,128)(2,1)}, u32[]{:S(2)}) copy-start(bf16[2,64,128]{2,1,0:T(8,128)(2,1)} %param.10) | copy-start | bytes 98308
  170.9 14.5 %copy-start.8 = (bf16[128]{0:T(256)(128)(2,1)S(1)}, bf16[128]{0:T(256)(128)(2,1)}, u32[]{:S(2)}) copy-start(bf16[128]{0:T(256)(128)(2,1)} %param.19) | copy-start | bytes 772
  180.5 14.6 %all-to-all-start.6 = ((bf16[32,2,128]{2,1,0:T(2,128)(2,1)}), bf16[32,2,128]{2,1,0:T(2,128)(2,1)S(1)}, u32[]{:S(2)}, u32[]{:S(2)}) async-start(bf16[32,2,128]{2,1,0:T(2,128)(2,1)} %broadcast_in_dim.121), calls=%async_computation.6 | async-start | bytes 32768 | tf_op jit(solution)/shard_map/all_to_all | solution.py:17

commit v2 on v1

v2 whole, which is shorter than its diff:
```python
import jax
import jax.numpy as jnp
from jax import lax
from jax.sharding import Mesh
from jax.sharding import PartitionSpec as P

D = 4096
LAYERS = 2
LANES = 128
EPS = 1e-06
F32 = jnp.float32
BF16 = jnp.bfloat16
TN = (((0,), (0,)), ((), ()))


def exchanged(x, axis):
    return lax.all_to_all(x, axis, split_axis=0, concat_axis=0, tiled=True)


def to_everyone(x, axis):
    copies = jnp.broadcast_to(x[None], (lax.axis_size(axis), *x.shape))
    return exchanged(copies, axis)


def two_halves(row):
    high = row.astype(BF16)
    low = (row - high.astype(F32)).astype(BF16)
    return jnp.concatenate([high, low], axis=0)


def shifted(x, by, position):
    moved = jnp.pad(x, ((0, 0), (by, 0)))[:, : x.shape[1]]
    return jnp.where(position >= by, moved, 0.0)


def causal_mix(rows, columns, position):
    x = rows.astype(F32)
    return (
        columns[:, 3:4]
        + shifted(x, 2, position) * columns[:, 0:1]
        + shifted(x, 1, position) * columns[:, 1:2]
        + x * columns[:, 2:3]
    )


def in_tiles(weight):
    rows, columns = weight.shape
    return weight.reshape(rows, columns // LANES, LANES).swapaxes(0, 1)


def body(
    stream,
    norm_gain,
    gate_weight,
    value_weight,
    gate_taps,
    value_taps,
    gate_bias,
    value_bias,
    down_weight,
    final_gain,
):
    batch_rows, length, width = stream.shape
    tokens = batch_rows * length
    ny, nx, nz = lax.axis_size("y"), lax.axis_size("x"), lax.axis_size("z")
    ff = gate_weight.shape[2]
    block = ff // ny
    units = block // nz
    half = block // 2
    core = lax.axis_index("dp")
    plane = ("y", "x")
    members = nx * ny
    piece = tokens // members
    position = lax.broadcasted_iota(jnp.int32, (1, tokens), 1) % length

    first = core == 0
    sent = [
        jnp.broadcast_to(stream.reshape(1, tokens, width), (ny, tokens, width)),
        jnp.broadcast_to(jnp.pad(norm_gain, ((0, 14), (0, 0)))[None], (ny, 16, width)),
    ]
    for layer in range(LAYERS):
        up = in_tiles(jnp.where(first, gate_weight[layer], value_weight[layer]))
        sent.append(up.reshape(ny, -1, LANES))
        down = down_weight[layer].reshape(ny, 2, half, width)
        sent.append(lax.dynamic_index_in_dim(down, core, 1, keepdims=False))
    ends, at = [], 0
    for a in sent[:-1]:
        at += a.shape[1]
        ends.append(at)
    mine = exchanged(jnp.concatenate(sent, axis=1), "y")
    other = lax.ppermute(mine, "dp", [(0, 1), (1, 0)])
    mine = jnp.split(mine, ends, axis=1)
    other = jnp.split(other, ends, axis=1)

    lower = lax.axis_index("y") * block + lax.axis_index("z") * units
    table = jnp.concatenate(
        [gate_taps, gate_bias[:, None], value_taps, value_bias[:, None]], axis=1
    )
    table = lax.dynamic_slice_in_dim(table, lower, units, 2)
    table = jnp.swapaxes(table, 1, 2).astype(F32)
    gains = mine[1].astype(F32)
    place = lax.axis_index(plane)

    current = mine[0]
    for layer in range(LAYERS):
        values = current.astype(F32)
        squares = jnp.sum(values * values, axis=(0, 2))[None]
        gained = (values * gains[:, layer][:, None]).astype(BF16)
        gained = gained.swapaxes(0, 1).reshape(tokens, ny * width)

        def projected(tiles):
            tiles = tiles.reshape(ny, block // LANES, width, LANES)
            weight = tiles.transpose(0, 2, 1, 3).reshape(ny * width, block)
            out = jnp.dot(gained, weight, preferred_element_type=F32).astype(BF16)
            return out.T.reshape(nz, units, tokens)

        a, b = projected(mine[2 + 2 * layer]), projected(other[2 + 2 * layer])
        parts = jnp.concatenate(
            [
                jnp.where(first, a, b),
                jnp.where(first, b, a),
                jnp.broadcast_to(jnp.pad(two_halves(squares), ((0, 6), (0, 0)))[None], (nz, 8, tokens)),
            ],
            axis=1,
        )
        total = exchanged(parts, "z").astype(F32).sum(axis=0)
        scale = lax.rsqrt((total[2 * units] + total[2 * units + 1])[None] / D + EPS)
        gate_up = (total[:units] * scale).astype(BF16)
        value_up = (total[units : 2 * units] * scale).astype(BF16)
        gate_conv = causal_mix(gate_up, table[layer, :, 0:4], position)
        value_conv = causal_mix(value_up, table[layer, :, 4:8], position)
        hidden = (jax.nn.gelu(gate_conv) * value_conv).astype(BF16)
        gathered = to_everyone(hidden, "z").reshape(2, half, tokens)
        down = (mine[3 + 2 * layer], other[3 + 2 * layer])
        term = 0.0
        for k in range(2):
            rows = lax.dynamic_index_in_dim(gathered, core if k == 0 else 1 - core, 0, keepdims=False)
            term = term + jnp.einsum("ut,yud->ytd", rows, down[k], preferred_element_type=F32)
        term = term.astype(BF16)
        if layer < LAYERS - 1:
            term = term.reshape(ny, members, piece, width).swapaxes(0, 1)
            summed = exchanged(term, plane).astype(F32).sum(axis=0)
            own = lax.dynamic_slice_in_dim(values, place * piece, piece, 1)
            fresh = (0.5 * own + summed).astype(BF16)
            current = to_everyone(fresh, plane).swapaxes(0, 1).reshape(ny, tokens, width)
        else:
            term = jnp.broadcast_to(term[:, None], (ny, nx, tokens, width)).reshape(members, tokens, width)
            branch = exchanged(term, plane).astype(F32).sum(axis=0)
            own = lax.dynamic_index_in_dim(values, lax.axis_index("y"), 0, keepdims=False)
            last = (0.5 * own + branch).astype(BF16).astype(F32)
    squares = jnp.sum(last * last, axis=1)[None]
    total = to_everyone(two_halves(squares), ("z", "y")).astype(F32).sum(axis=(0, 1))
    mixed = last * lax.rsqrt(total[:, None] / D + EPS) * final_gain.astype(F32)[None]
    return mixed.astype(BF16).reshape(batch_rows, length, width)


def solution(mesh):
    split = Mesh(
        mesh.devices.reshape(8, 4, mesh.shape["cb"], mesh.shape["dp"]), ("z", "y", "x", "dp")
    )
    ra = ("z", "y")
    return jax.shard_map(
        body,
        mesh=split,
        in_specs=(
            P("dp", None, ra),
            P(None, ra),
            P(None, ra, "x"),
            P(None, ra, "x"),
            P(None, None, "x"),
            P(None, None, "x"),
            P(None, "x"),
            P(None, "x"),
            P(None, "x", ra),
            P(ra),
        ),
        out_specs=P("dp", None, ra),
        check_vma=False,
    )
```

time: 197 us -> 191 us (0.970)
  waiting for transfers between devices: 91.6 us -> 65.9 us
  local copies, waits for them, and re-layouts: 3.58 us -> 24 us
  blocking collectives: 61.8 us -> 47.4 us
  starting transfers between devices: 26.4 us -> 34.2 us
  matrix products: 5.86 us -> 8.91 us
  other arithmetic: 6.07 us -> 8.7 us
    all_to_all x4 -> x7, waiting for transfers between devices: 91.6 us -> 65 us  [exchanged(): return lax.all_to_all(x, axis, split_axis=0, concat_axis=0, tiled=True)]
    all_to_all x3 -> x2, blocking collectives: 61.8 us -> 47.4 us  [exchanged(): return lax.all_to_all(x, axis, split_axis=0, concat_axis=0, tiled=True)]
    reshape x0 -> x5, local copies, waits for them, and re-layouts: none -> 8.61 us  [the longest x4 7.95 us: projected(): tiles = tiles.reshape(ny, block // LANES, width, LANES)]
    all_to_all x4 -> x7, starting transfers between devices: 26.4 us -> 34.2 us  [exchanged(): return lax.all_to_all(x, axis, split_axis=0, concat_axis=0, tiled=True)]
    unnamed x18 -> x37, local copies, waits for them, and re-layouts: 0.03 us -> 5.15 us
    split x0 -> x2, local copies, waits for them, and re-layouts: none -> 3.63 us  [the longest x1 2.65 us: body(): other = jnp.split(other, ends, axis=1)]
    dot_general x6 -> x8, matrix products: 5.86 us -> 8.91 us  [the longest x4 5.8 us: projected(): out = jnp.dot(gained, weight, preferred_element_type=F32).astype(BF16)]
    unnamed x0 -> x1, other arithmetic: none -> 2 us
  transfers between devices with their start and end apart: 4 -> 8, of which waited for: 4 -> 8; matrix products, arithmetic and copies ran while one was open for 0% -> 5% of each run, Pallas kernels for 0% -> 0%
where the time goes in v2:
time: 191 us; the launch traced here: 189 us
  waiting for transfers between devices  65.9 us (35%)
  blocking collectives  47.4 us (25%)
  starting transfers between devices  34.2 us (18%)
  local copies, waits for them, and re-layouts  24 us (13%)
  matrix products  8.91 us (5%)
  other arithmetic  8.7 us (5%)
    all_to_all x7, waiting for transfers between devices, exchanged(): return lax.all_to_all(x, axis, split_axis=0, concat_axis=0, tiled=True)  65 us
    all_to_all x2, blocking collectives, exchanged(): return lax.all_to_all(x, axis, split_axis=0, concat_axis=0, tiled=True)  47.4 us
    all_to_all x7, starting transfers between devices, exchanged(): return lax.all_to_all(x, axis, split_axis=0, concat_axis=0, tiled=True)  34.2 us
    reshape x4, local copies, waits for them, and re-layouts, projected(): tiles = tiles.reshape(ny, block // LANES, width, LANES)  7.95 us
    dot_general x4, matrix products, projected(): out = jnp.dot(gained, weight, preferred_element_type=F32).astype(BF16)  5.8 us
    unnamed x37, local copies, waits for them, and re-layouts  5.15 us
  transfers between devices with their start and end apart: 8, of which 8 were waited for; matrix products, arithmetic and copies ran while one was open for 5% of the time, Pallas kernels for 0%

profile of v2, /device:TPU:2, one launch (start us, length us, event | category | flops | bytes accessed | tf_op | source)
XLA Modules:
  0.0 189.4 jit_solution(9835329781693189815)
XLA Ops:
  0.0 2.0 %select_bitcast_fusion = (bf16[16,8,24,128]{3,1,2,0:T(8,128)(2,1)S(1)}, bf16[16,8,24,128]{3,1,2,0:T(8,128)(2,1)S(1)}) fusion(bf16[2,128,3072]{2,1,0:T(8,128)(2,1)} %param.13, bf16[2,128,3072]{2,1,0:T(8,128)(2,1)} %param.12, pred[]{:T(512)S(6)} %eq.5), kind=kLoop, calls=%fused_computation.21 | loop fusion | flops 786432 | bytes 4718593
  2.8 0.7 broadcast_dynamic-update-slice_fusion
  4.7 1.0 constant_dynamic-update-slice_fusion.1
  5.7 0.8 bitcast_dynamic-update-slice_fusion.1
  6.6 1.0 constant_dynamic-update-slice_fusion
  7.6 0.8 bitcast_dynamic-update-slice_fusion
  8.4 35.2 %all_to_all.45 = bf16[4,2448,128]{2,1,0:T(8,128)(2,1)S(1)} all-to-all(bf16[4,2448,128]{2,1,0:T(8,128)(2,1)} %bitcast_dynamic-update-slice_fusion), channel_id=1, replica_groups=mesh['z'=8,'y'=4,'x'=4,'dp'=2] {'y'}, dimensions={0} | all-to-all | bytes 5013504 | tf_op jit(solution)/shard_map/all_to_all | solution.py:17
  44.5 1.0 fusion.101
  45.5 2.2 %copy.106 = bf16[4,6,128,128]{2,0,3,1:T(4,128)(2,1)} copy(bf16[4,6,128,128]{3,2,1,0:T(8,128)(2,1)} %bitcast.189) | data formatting | bytes 1572864 | tf_op jit(solution)/shard_map/reshape | solution.py:112
  47.7 0.8 collective-permute-done
  48.5 2.6 %fusion.102 = (bf16[4,768,128]{2,1,0:T(8,128)(2,1)}, bf16[4,768,128]{2,1,0:T(8,128)(2,1)}) fusion(bf16[4,2448,128]{2,1,0:T(8,128)(2,1)} %collective-permute-done), kind=kLoop, calls=%fused_computation.191 | loop fusion | bytes 3145728 | tf_op jit(solution)/shard_map/split | solution.py:93
  51.1 2.2 %copy.108 = bf16[4,6,128,128]{2,0,3,1:T(4,128)(2,1)} copy(bf16[4,6,128,128]{3,2,1,0:T(8,128)(2,1)} %bitcast.190) | data formatting | bytes 1572864 | tf_op jit(solution)/shard_map/reshape | solution.py:112
  53.4 1.5 convolution_convert_fusion.2
  54.9 1.5 broadcast_select_fusion.3
  56.4 0.8 pad_maximum_fusion
  57.2 8.5 %all-to-all-start.1 = ((bf16[8,200,128]{2,1,0:T(8,128)(2,1)}), bf16[8,200,128]{2,1,0:T(8,128)(2,1)}, u32[]{:S(2)}, u32[]{:S(2)}) async-start(bf16[8,200,128]{2,1,0:T(8,128)(2,1)} %pad_maximum_fusion), calls=%async_computation.1 | async-start | bytes 819200 | tf_op jit(solution)/shard_map/all_to_all | solution.py:17
  66.4 14.7 %all-to-all-done.1 = bf16[8,200,128]{2,1,0:T(8,128)(2,1)} async-done(((bf16[8,200,128]{2,1,0:T(8,128)(2,1)}), bf16[8,200,128]{2,1,0:T(8,128)(2,1)}, u32[]{:S(2)}, u32[]{:S(2)}) %all-to-all-start.1) | async-done | bytes 409632 | tf_op jit(solution)/shard_map/all_to_all | solution.py:17
  81.1 1.1 convert_reduce_fusion.2
  82.4 0.7 broadcast_in_dim.131
  83.2 3.4 %all-to-all-start.2 = ((bf16[8,96,128]{2,1,0:T(8,128)(2,1)}), bf16[8,96,128]{2,1,0:T(8,128)(2,1)S(1)}, u32[]{:S(2)}, u32[]{:S(2)}) async-start(bf16[8,96,128]{2,1,0:T(8,128)(2,1)} %broadcast_in_dim.131), calls=%async_computation.2 | async-start | bytes 393216 | tf_op jit(solution)/shard_map/all_to_all | solution.py:17
  86.6 10.8 %all-to-all-done.2 = bf16[8,96,128]{2,1,0:T(8,128)(2,1)S(1)} async-done(((bf16[8,96,128]{2,1,0:T(8,128)(2,1)}), bf16[8,96,128]{2,1,0:T(8,128)(2,1)S(1)}, u32[]{:S(2)}, u32[]{:S(2)}) %all-to-all-start.2) | async-done | bytes 196640 | tf_op jit(solution)/shard_map/all_to_all | solution.py:17
  97.7 1.3 fusion.2
  98.9 0.7 copy.156
  99.6 5.4 %all-to-all-start.3 = ((bf16[16,4,8,128]{3,2,1,0:T(8,128)(2,1)}), bf16[16,4,8,128]{3,2,1,0:T(8,128)(2,1)S(1)}, u32[]{:S(2)}, u32[]{:S(2)}) async-start(bf16[16,4,8,128]{3,2,1,0:T(8,128)(2,1)} %bitcast.182), calls=%async_computation.3 | async-start | bytes 262144 | tf_op jit(solution)/shard_map/all_to_all | solution.py:17
  105.0 0.7 slice_convert_fusion
  105.7 5.9 %all-to-all-done.3 = bf16[16,4,8,128]{3,2,1,0:T(8,128)(2,1)S(1)} async-done(((bf16[16,4,8,128]{3,2,1,0:T(8,128)(2,1)}), bf16[16,4,8,128]{3,2,1,0:T(8,128)(2,1)S(1)}, u32[]{:S(2)}, u32[]{:S(2)}) %all-to-all-start.3) | async-done | bytes 131104 | tf_op jit(solution)/shard_map/all_to_all | solution.py:17
  111.7 0.7 add_convert_fusion.1
  112.4 0.7 broadcast_in_dim.132
  113.1 4.8 %all-to-all-start.4 = ((bf16[16,4,8,128]{3,2,1,0:T(8,128)(2,1)}), bf16[16,4,8,128]{3,2,1,0:T(8,128)(2,1)S(1)}, u32[]{:S(2)}, u32[]{:S(2)}) async-start(bf16[16,4,8,128]{3,2,1,0:T(8,128)(2,1)} %broadcast_in_dim.132), calls=%async_computation.4 | async-start | bytes 262144 | tf_op jit(solution)/shard_map/all_to_all | solution.py:17
  117.8 1.3 copy.113
  119.1 2.3 %copy.115 = bf16[4,6,128,128]{2,0,3,1:T(4,128)(2,1)} copy(bf16[4,6,128,128]{3,2,1,0:T(8,128)(2,1)} %bitcast.188) | data formatting | bytes 1572864 | tf_op jit(solution)/shard_map/reshape | solution.py:112
  121.4 3.2 %all-to-all-done.4 = bf16[16,4,8,128]{3,2,1,0:T(8,128)(2,1)S(1)} async-done(((bf16[16,4,8,128]{3,2,1,0:T(8,128)(2,1)}), bf16[16,4,8,128]{3,2,1,0:T(8,128)(2,1)S(1)}, u32[]{:S(2)}, u32[]{:S(2)}) %all-to-all-start.4) | async-done | bytes 131104 | tf_op jit(solution)/shard_map/all_to_all | solution.py:17
  124.5 0.7 fusion.20
  125.3 0.8 copy.114
  126.2 1.5 convolution_convert_fusion
  127.8 1.3 broadcast_select_fusion.1
  129.1 0.8 pad_maximum_fusion.1
  129.9 3.5 %all-to-all-start.5 = ((bf16[8,200,128]{2,1,0:T(8,128)(2,1)}), bf16[8,200,128]{2,1,0:T(8,128)(2,1)S(1)}, u32[]{:S(2)}, u32[]{:S(2)}) async-start(bf16[8,200,128]{2,1,0:T(8,128)(2,1)} %pad_maximum_fusion.1), calls=%async_computation.5 | async-start | bytes 819200 | tf_op jit(solution)/shard_map/all_to_all | solution.py:17
  133.4 11.9 %all-to-all-done.5 = bf16[8,200,128]{2,1,0:T(8,128)(2,1)S(1)} async-done(((bf16[8,200,128]{2,1,0:T(8,128)(2,1)}), bf16[8,200,128]{2,1,0:T(8,128)(2,1)S(1)}, u32[]{:S(2)}, u32[]{:S(2)}) %all-to-all-start.5) | async-done | bytes 409632 | tf_op jit(solution)/shard_map/all_to_all | solution.py:17
  145.7 12.2 %all_to_all.46 = bf16[8,96,128]{2,1,0:T(8,128)(2,1)S(1)} all-to-all(bf16[8,96,128]{2,1,0:T(8,128)(2,1)S(1)} %broadcast_in_dim.134), channel_id=1, replica_groups=mesh['z'=8,'y'=4,'x'=4,'dp'=2] {'z'}, dimensions={0} | all-to-all | bytes 393216 | tf_op jit(solution)/shard_map/all_to_all | solution.py:17
  158.2 1.3 fusion.3
  159.6 0.9 broadcast_in_dim.135
  160.5 4.8 %all-to-all-start.7 = ((bf16[16,128,128]{2,1,0:T(8,128)(2,1)}), bf16[16,128,128]{2,1,0:T(8,128)(2,1)S(1)}, u32[]{:S(2)}, u32[]{:S(2)}) async-start(bf16[16,128,128]{2,1,0:T(8,128)(2,1)} %bitcast.71), calls=%async_computation.7 | async-start | bytes 1048576 | tf_op jit(solution)/shard_map/all_to_all | solution.py:17
  165.3 8.8 %all-to-all-done.7 = bf16[16,128,128]{2,1,0:T(8,128)(2,1)S(1)} async-done(((bf16[16,128,128]{2,1,0:T(8,128)(2,1)}), bf16[16,128,128]{2,1,0:T(8,128)(2,1)S(1)}, u32[]{:S(2)}, u32[]{:S(2)}) %all-to-all-start.7) | async-done | bytes 524320 | tf_op jit(solution)/shard_map/all_to_all | solution.py:17
  174.4 0.6 broadcast_in_dim.136
  175.0 3.8 %all-to-all-start.8 = ((bf16[32,2,128]{2,1,0:T(2,128)(2,1)}), bf16[32,2,128]{2,1,0:T(2,128)(2,1)S(1)}, u32[]{:S(2)}, u32[]{:S(2)}) async-start(bf16[32,2,128]{2,1,0:T(2,128)(2,1)} %broadcast_in_dim.136), calls=%async_computation.8 | async-start | bytes 32768 | tf_op jit(solution)/shard_map/all_to_all | solution.py:17
  178.9 9.7 %all-to-all-done.8 = bf16[32,2,128]{2,1,0:T(2,128)(2,1)S(1)} async-done(((bf16[32,2,128]{2,1,0:T(2,128)(2,1)}), bf16[32,2,128]{2,1,0:T(2,128)(2,1)S(1)}, u32[]{:S(2)}, u32[]{:S(2)}) %all-to-all-start.8) | async-done | bytes 16416 | tf_op jit(solution)/shard_map/all_to_all | solution.py:17
  188.7 0.7 multiply_convert_fusion.2
  (78 shorter events, 5.4 us)
Async XLA Ops:
  2.0 0.8 copy-start.4
  2.0 1.4 copy-start
  3.4 0.7 copy-start.13
  43.6 4.9 %collective-permute-start = (bf16[4,2448,128]{2,1,0:T(8,128)(2,1)S(1)}, bf16[4,2448,128]{2,1,0:T(8,128)(2,1)}, u32[]{:S(2)}, u32[]{:S(2)}) collective-permute-start(bf16[4,2448,128]{2,1,0:T(8,128)(2,1)S(1)} %all_to_all.45), channel_id=1, source_target_pairs={{0,1},{1,0},{2,3},{3,2},{4,5},{5,4},{6,7},{7,6},{8,9},{9,8},{10,11... | collective-permute-start | bytes 7520264 | tf_op jit(solution)/shard_map/ppermute | solution.py:91
  53.3 12.3 %copy-start.2 = (bf16[2,3,3072]{2,0,1:T(2,128)(2,1)S(1)}, bf16[2,3,3072]{2,0,1:T(2,128)(2,1)}, u32[]{:S(2)}) copy-start(bf16[2,3,3072]{2,0,1:T(2,128)(2,1)} %param.15) | copy-start | bytes 110596
  53.3 12.3 %copy-start.3 = (bf16[2,3,3072]{2,0,1:T(2,128)(2,1)S(1)}, bf16[2,3,3072]{2,0,1:T(2,128)(2,1)}, u32[]{:S(2)}) copy-start(bf16[2,3,3072]{2,0,1:T(2,128)(2,1)} %param.14) | copy-start | bytes 110596
  53.4 12.4 %copy-start.5 = (bf16[2,3072]{1,0:T(2,128)(2,1)S(1)}, bf16[2,3072]{1,0:T(2,128)(2,1)}, u32[]{:S(2)}) copy-start(bf16[2,3072]{1,0:T(2,128)(2,1)} %param.17) | copy-start | bytes 36868
  53.4 12.4 %copy-start.6 = (bf16[2,3072]{1,0:T(2,128)(2,1)S(1)}, bf16[2,3072]{1,0:T(2,128)(2,1)}, u32[]{:S(2)}) copy-start(bf16[2,3072]{1,0:T(2,128)(2,1)} %param.16) | copy-start | bytes 36868
  57.2 23.9 %all-to-all-start.1 = ((bf16[8,200,128]{2,1,0:T(8,128)(2,1)}), bf16[8,200,128]{2,1,0:T(8,128)(2,1)}, u32[]{:S(2)}, u32[]{:S(2)}) async-start(bf16[8,200,128]{2,1,0:T(8,128)(2,1)} %pad_maximum_fusion), calls=%async_computation.1 | async-start | bytes 819200 | tf_op jit(solution)/shard_map/all_to_all | solution.py:17
  65.7 17.5 %copy-start.9 = (pred[128]{0:T(512)(128)(4,1)}, pred[128]{0:T(512)(128)(4,1)S(1)}, u32[]{:S(2)}) copy-start(pred[128]{0:T(512)(128)(4,1)S(1)} %get-tuple-element.49) | copy-start | bytes 388
  65.7 17.5 %copy-start.11 = (pred[128]{0:T(512)(128)(4,1)}, pred[128]{0:T(512)(128)(4,1)S(1)}, u32[]{:S(2)}) copy-start(pred[128]{0:T(512)(128)(4,1)S(1)} %get-tuple-element.50) | copy-start | bytes 388
  83.2 14.2 %all-to-all-start.2 = ((bf16[8,96,128]{2,1,0:T(8,128)(2,1)}), bf16[8,96,128]{2,1,0:T(8,128)(2,1)S(1)}, u32[]{:S(2)}, u32[]{:S(2)}) async-start(bf16[8,96,128]{2,1,0:T(8,128)(2,1)} %broadcast_in_dim.131), calls=%async_computation.2 | async-start | bytes 393216 | tf_op jit(solution)/shard_map/all_to_all | solution.py:17
  99.6 12.1 %all-to-all-start.3 = ((bf16[16,4,8,128]{3,2,1,0:T(8,128)(2,1)}), bf16[16,4,8,128]{3,2,1,0:T(8,128)(2,1)S(1)}, u32[]{:S(2)}, u32[]{:S(2)}) async-start(bf16[16,4,8,128]{3,2,1,0:T(8,128)(2,1)} %bitcast.182), calls=%async_computation.3 | async-start | bytes 262144 | tf_op jit(solution)/shard_map/all_to_all | solution.py:17
  113.1 11.5 %all-to-all-start.4 = ((bf16[16,4,8,128]{3,2,1,0:T(8,128)(2,1)}), bf16[16,4,8,128]{3,2,1,0:T(8,128)(2,1)S(1)}, u32[]{:S(2)}, u32[]{:S(2)}) async-start(bf16[16,4,8,128]{3,2,1,0:T(8,128)(2,1)} %broadcast_in_dim.132), calls=%async_computation.4 | async-start | bytes 262144 | tf_op jit(solution)/shard_map/all_to_all | solution.py:17
  119.1 8.7 %copy-start.1 = (bf16[4,6,128,128]{2,0,3,1:T(4,128)(2,1)S(1)}, bf16[4,6,128,128]{2,0,3,1:T(4,128)(2,1)}, u32[]{:S(2)}) copy-start(bf16[4,6,128,128]{2,0,3,1:T(4,128)(2,1)} %copy.113) | copy-start | bytes 2359300
  126.0 7.3 %copy-start.7 = (f32[1,96,4]{1,0,2:T(1,128)S(1)}, f32[1,96,4]{1,0,2:T(1,128)}, u32[]{:S(2)}) copy-start(f32[1,96,4]{1,0,2:T(1,128)} %get-tuple-element.27) | copy-start | bytes 4612
  126.0 7.3 %copy-start.8 = (f32[1,96,4]{1,0,2:T(1,128)S(1)}, f32[1,96,4]{1,0,2:T(1,128)}, u32[]{:S(2)}) copy-start(f32[1,96,4]{1,0,2:T(1,128)} %get-tuple-element.28) | copy-start | bytes 4612
  126.2 19.2 %copy-start.10 = (pred[128]{0:T(512)(128)(4,1)S(1)}, pred[128]{0:T(512)(128)(4,1)}, u32[]{:S(2)}) copy-start(pred[128]{0:T(512)(128)(4,1)} %copy-done.9) | copy-start | bytes 388
  126.2 19.2 %copy-start.12 = (pred[128]{0:T(512)(128)(4,1)S(1)}, pred[128]{0:T(512)(128)(4,1)}, u32[]{:S(2)}) copy-start(pred[128]{0:T(512)(128)(4,1)} %copy-done.11) | copy-start | bytes 388
  129.9 15.4 %all-to-all-start.5 = ((bf16[8,200,128]{2,1,0:T(8,128)(2,1)}), bf16[8,200,128]{2,1,0:T(8,128)(2,1)S(1)}, u32[]{:S(2)}, u32[]{:S(2)}) async-start(bf16[8,200,128]{2,1,0:T(8,128)(2,1)} %pad_maximum_fusion.1), calls=%async_computation.5 | async-start | bytes 819200 | tf_op jit(solution)/shard_map/all_to_all | solution.py:17
  157.8 21.0 %copy-start.14 = (bf16[128]{0:T(256)(128)(2,1)S(1)}, bf16[128]{0:T(256)(128)(2,1)}, u32[]{:S(2)}) copy-start(bf16[128]{0:T(256)(128)(2,1)} %param.19) | copy-start | bytes 772
  160.5 13.7 %all-to-all-start.7 = ((bf16[16,128,128]{2,1,0:T(8,128)(2,1)}), bf16[16,128,128]{2,1,0:T(8,128)(2,1)S(1)}, u32[]{:S(2)}, u32[]{:S(2)}) async-start(bf16[16,128,128]{2,1,0:T(8,128)(2,1)} %bitcast.71), calls=%async_computation.7 | async-start | bytes 1048576 | tf_op jit(solution)/shard_map/all_to_all | solution.py:17
  175.0 13.5 %all-to-all-start.8 = ((bf16[32,2,128]{2,1,0:T(2,128)(2,1)}), bf16[32,2,128]{2,1,0:T(2,128)(2,1)S(1)}, u32[]{:S(2)}, u32[]{:S(2)}) async-start(bf16[32,2,128]{2,1,0:T(2,128)(2,1)} %broadcast_in_dim.136), calls=%async_computation.8 | async-start | bytes 32768 | tf_op jit(solution)/shard_map/all_to_all | solution.py:17

commit v3 on v1

v3 whole, which is shorter than its diff:
```python
import functools

import jax
import jax.numpy as jnp
from jax import lax
from jax.experimental import pallas as pl
from jax.experimental.pallas import tpu as pltpu
from jax.sharding import Mesh
from jax.sharding import PartitionSpec as P

D = 4096
LAYERS = 2
LANES = 128
EXTRA = 16
EPS = 1e-06
F32 = jnp.float32
BF16 = jnp.bfloat16
TN = (((0,), (0,)), ((), ()))
VMEM = pl.BlockSpec(memory_space=pltpu.VMEM)
ANY = pl.BlockSpec(memory_space=pl.ANY)


def exchanged(x, axis):
    return lax.all_to_all(x, axis, split_axis=0, concat_axis=0, tiled=True)


def to_everyone(x, axis):
    copies = jnp.broadcast_to(x[None], (lax.axis_size(axis), *x.shape))
    return exchanged(copies, axis)


def two_halves(row):
    high = row.astype(BF16)
    low = (row - high.astype(F32)).astype(BF16)
    return jnp.concatenate([high, low], axis=0)


def room(mebibytes):
    return pltpu.CompilerParams(vmem_limit_bytes=mebibytes * 1024 * 1024)


def cost(flops, moved):
    return pl.CostEstimate(flops=flops, bytes_accessed=moved, transcendentals=0)


def pack_kernel(layer, ny, start, *refs):
    if start:
        gate, value, stream, gain, out, sems = refs
    else:
        gate, value, out, sems = refs
    width = gate.shape[1]
    tiles = gate.shape[2] // LANES
    each = tiles // ny
    first = lax.axis_index("dp") == 0

    def copies(ref):
        for j in range(tiles):
            yield pltpu.make_async_copy(
                ref.at[layer, :, pl.ds(j * LANES, LANES)],
                out.at[j // each, pl.ds(start + (j % each) * width, width), :],
                sems.at[j],
            )

    @pl.when(first)
    def _():
        for c in copies(gate):
            c.start()

    @pl.when(jnp.logical_not(first))
    def _():
        for c in copies(value):
            c.start()

    if start:
        tokens = stream.shape[0]
        block = stream[...]
        gains = jnp.broadcast_to(gain[...].astype(F32)[:, None, :], (LAYERS, 8, width))
        gains = gains.reshape(LAYERS * 8, width).astype(BF16)
        for i in range(ny):
            out[i, 0:tokens, :] = block
            out[i, tokens : tokens + LAYERS * 8, :] = gains
    for c in copies(gate):
        c.wait()


def packed(layer, ny, gate, value, stream=None, gain=None):
    width, columns = gate.shape[1:]
    rows = columns // ny // LANES * width
    start = 0 if stream is None else stream.shape[0] + LAYERS * 8
    args = (gate, value) if stream is None else (gate, value, stream, gain)
    specs = [ANY, ANY] if stream is None else [ANY, ANY, VMEM, VMEM]
    return pl.pallas_call(
        functools.partial(pack_kernel, layer, ny, start),
        out_shape=jax.ShapeDtypeStruct((ny, start + rows, LANES), BF16),
        in_specs=specs,
        out_specs=VMEM,
        scratch_shapes=[pltpu.SemaphoreType.DMA((columns // LANES,))],
        cost_estimate=cost(1000000, 2 * width * columns * 2),
        compiler_params=room(4),
        name=f"pack{layer}",
    )(*args)


def up_kernel(layer, start, ny, nx, nz, *refs):
    if layer == 0:
        mine, other, out = refs
        first_mine = mine
        weights = [(mine.at[k], other.at[k]) for k in range(ny)]
    else:
        first_mine, terms = refs[0], refs[1]
        weights = [(refs[2 + k], refs[2 + ny + k]) for k in range(ny)]
        out, kept = refs[2 + 2 * ny :]
    tokens = LANES
    width = LANES
    block = weights[0][0].shape[0] - start
    units = block // nz
    core = lax.axis_index("dp")
    y = lax.axis_index("y")
    squares = jnp.zeros((tokens, LANES), F32)
    gained = []
    for k in range(ny):
        at = k if layer == 0 else lax.rem(y - k + ny, ny)
        values = first_mine[at, 0:tokens, :].astype(F32)
        if layer:
            branch = terms[at * nx].astype(F32)
            for i in range(1, nx):
                branch = branch + terms[at * nx + i].astype(F32)
            rounded = (0.5 * values + branch).astype(BF16)
            if k == 0:
                kept[...] = rounded
            values = rounded.astype(F32)
        gain = first_mine[at, tokens : tokens + 16, :].astype(F32)[8 * layer : 8 * layer + 1]
        squares = squares + values * values
        gained.append((values * gain).astype(BF16))
    gained = jnp.concatenate(gained, axis=1)
    for side in range(2):
        rows = pl.multiple_of((core if side == 0 else 1 - core) * units, 16)
        for j in range(block // LANES):
            weight = jnp.concatenate(
                [w[side][pl.ds(start + j * width, width), :] for w in weights], axis=0
            )
            result = jnp.dot(gained, weight, preferred_element_type=F32).T.astype(BF16)
            low = j * LANES
            while low < (j + 1) * LANES:
                slot = low // units
                high = min((j + 1) * LANES, (slot + 1) * units)
                out[slot, pl.ds(rows + (low - slot * units), high - low), :] = result[
                    low - j * LANES : high - j * LANES
                ]
                low = high
    total = jnp.broadcast_to(jnp.sum(squares, axis=1, keepdims=True), (tokens, LANES)).T[0:EXTRA]
    high = total.astype(BF16).astype(F32)
    index = lax.broadcasted_iota(jnp.int32, (EXTRA, LANES), 0)
    both = jnp.where(index == 0, high, jnp.where(index == 1, total - high, 0.0)).astype(BF16)
    for i in range(nz):
        out[i, 2 * units : 2 * units + EXTRA, :] = both


def projected(layer, start, block, ny, nx, nz, args):
    units = block // nz
    shapes = [jax.ShapeDtypeStruct((nz, 2 * units + EXTRA, LANES), BF16)]
    if layer:
        shapes.append(jax.ShapeDtypeStruct((LANES, LANES), BF16))
    return pl.pallas_call(
        functools.partial(up_kernel, layer, start, ny, nx, nz),
        out_shape=shapes,
        in_specs=[VMEM] * len(args),
        out_specs=[VMEM] * len(shapes),
        cost_estimate=cost(4 * ny * LANES * LANES * block, 4 * ny * LANES * block),
        compiler_params=room(8),
        name=f"up{layer}",
    )(*args)


def mid_kernel(length, parts, table, out):
    count, rows, tokens = parts.shape
    units = out.shape[1]
    total = parts[0].astype(F32)
    for i in range(1, count):
        total = total + parts[i].astype(F32)
    mean = (total[2 * units : 2 * units + 1] + total[2 * units + 1 : 2 * units + 2]) / D
    scale = lax.rsqrt(mean + EPS)
    position = lax.rem(lax.broadcasted_iota(jnp.int32, (units, tokens), 1), length)
    columns = table[...]

    def mixed(low, at):
        x = (total[low : low + units] * scale).astype(BF16).astype(F32)
        one = jnp.where(position >= 1, pltpu.roll(x, 1, 1), 0.0)
        two = jnp.where(position >= 2, pltpu.roll(x, 2, 1), 0.0)
        return (
            columns[:, at + 3 : at + 4]
            + two * columns[:, at : at + 1]
            + one * columns[:, at + 1 : at + 2]
            + x * columns[:, at + 2 : at + 3]
        )

    hidden = (jax.nn.gelu(mixed(0, 0)) * mixed(units, 4)).astype(BF16)
    for i in range(out.shape[0]):
        out[i] = hidden


def gated(parts, table, length, copies):
    units = table.shape[0]
    return pl.pallas_call(
        functools.partial(mid_kernel, length),
        out_shape=jax.ShapeDtypeStruct((copies, units, parts.shape[2]), BF16),
        in_specs=[VMEM] * 2,
        out_specs=VMEM,
        cost_estimate=cost(1000000, parts.size * 2),
        compiler_params=room(6),
        name="mid",
    )(parts, table)


def down_kernel(hidden, weight, out):
    term = lax.dot_general(hidden[...], weight[0], TN, preferred_element_type=F32).astype(BF16)
    for i in range(out.shape[0]):
        out[i] = term


def lowered(layer, hidden, weight, copies):
    rows, width = weight.shape[1:]
    return pl.pallas_call(
        down_kernel,
        grid=(1,),
        out_shape=jax.ShapeDtypeStruct((copies, hidden.shape[1], width), BF16),
        in_specs=[
            pl.BlockSpec((rows, hidden.shape[1]), lambda i: (0, 0)),
            pl.BlockSpec((1, rows, width), lambda i: (layer, 0, 0)),
        ],
        out_specs=pl.BlockSpec((copies, hidden.shape[1], width), lambda i: (0, 0, 0)),
        cost_estimate=cost(2 * rows * width * hidden.shape[1], 4 * rows * width),
        compiler_params=room(8),
        name=f"down{layer}",
    )(hidden, weight)


def body(
    stream,
    norm_gain,
    gate_weight,
    value_weight,
    gate_taps,
    value_taps,
    gate_bias,
    value_bias,
    down_weight,
    final_gain,
):
    batch_rows, length, width = stream.shape
    tokens = batch_rows * length
    ny, nx, nz = lax.axis_size("y"), lax.axis_size("x"), lax.axis_size("z")
    block = gate_weight.shape[2] // ny
    units = block // nz
    start = tokens + LAYERS * 8
    swap = [(0, 1), (1, 0)]
    own = stream.reshape(tokens, width)

    mine = exchanged(packed(0, ny, gate_weight, value_weight, own, norm_gain), "y")
    other = lax.ppermute(mine, "dp", swap)
    later, mine = lax.optimization_barrier((packed(1, ny, gate_weight, value_weight), mine))
    y = lax.axis_index("y")
    near, far = [], []
    for k in range(ny):
        piece = lax.dynamic_index_in_dim(later, lax.rem(y + k, ny), 0, keepdims=False)
        if k:
            piece = lax.ppermute(piece, "y", [(i, (i + k) % ny) for i in range(ny)])
        near.append(piece)

    lower = y * block + lax.axis_index("z") * units
    table = jnp.concatenate(
        [gate_taps, gate_bias[:, None], value_taps, value_bias[:, None]], axis=1
    )
    table = lax.dynamic_slice_in_dim(table, lower, units, 2)
    table = jnp.swapaxes(table, 1, 2).astype(F32)

    (parts,) = projected(0, start, block, ny, nx, nz, [mine, other])
    parts, *near = lax.optimization_barrier((exchanged(parts, "z"), *near))
    far = [lax.ppermute(piece, "dp", swap) for piece in near]
    hidden = gated(parts, table[0], length, nz * ny)
    hidden = exchanged(hidden, ("y", "z")).reshape(-1, tokens)
    terms = exchanged(lowered(0, hidden, down_weight, ny * nx), ("y", "x"))

    parts, kept = projected(1, 0, block, ny, nx, nz, [mine, terms, *near, *far])
    hidden = gated(exchanged(parts, "z"), table[1], length, nz * ny)
    hidden = exchanged(hidden, ("y", "z")).reshape(-1, tokens)
    terms = exchanged(lowered(1, hidden, down_weight, nx), "x")
    branch = terms.astype(F32).sum(axis=0)
    last = (0.5 * kept.astype(F32) + branch).astype(BF16).astype(F32)
    squares = jnp.sum(last * last, axis=1)[None]
    total = to_everyone(two_halves(squares), ("z", "y")).astype(F32).sum(axis=(0, 1))
    mixed = last * lax.rsqrt(total[:, None] / D + EPS) * final_gain.astype(F32)[None]
    return mixed.astype(BF16).reshape(batch_rows, length, width)


def solution(mesh):
    split = Mesh(
        mesh.devices.reshape(8, 4, mesh.shape["cb"], mesh.shape["dp"]), ("z", "y", "x", "dp")
    )
    ra = ("z", "y")
    return jax.shard_map(
        body,
        mesh=split,
        in_specs=(
            P("dp", None, ra),
            P(None, ra),
            P(None, ra, "x"),
            P(None, ra, "x"),
            P(None, None, "x"),
            P(None, None, "x"),
            P(None, "x"),
            P(None, "x"),
            P(None, "x", ra),
            P(ra),
        ),
        out_specs=P("dp", None, ra),
        check_vma=False,
    )
```

time: 197 us -> 180 us (0.914)
  waiting for transfers between devices: 91.6 us -> 25.8 us
  blocking collectives: 61.8 us -> 104 us
  local copies, waits for them, and re-layouts: 3.58 us -> 17.8 us
  Pallas kernels: 0 us -> 6.39 us
  matrix products: 5.86 us -> 0 us
  other arithmetic: 6.07 us -> 1.89 us
  starting transfers between devices: 26.4 us -> 23.2 us
    all_to_all x4 -> x3, waiting for transfers between devices: 91.6 us -> 14.3 us  [exchanged(): return lax.all_to_all(x, axis, split_axis=0, concat_axis=0, tiled=True)]
    all_to_all x3 -> x5, blocking collectives: 61.8 us -> 104 us  [exchanged(): return lax.all_to_all(x, axis, split_axis=0, concat_axis=0, tiled=True)]
    unnamed x18 -> x38, local copies, waits for them, and re-layouts: 0.03 us -> 13.9 us
    ppermute x0 -> x8, waiting for transfers between devices: none -> 11.5 us  [the longest x3 9.06 us: body(): piece = lax.ppermute(piece, 'y', [(i, (i + k) % ny) for i in range(ny)])]
    all_to_all x4 -> x3, starting transfers between devices: 26.4 us -> 18.3 us  [exchanged(): return lax.all_to_all(x, axis, split_axis=0, concat_axis=0, tiled=True)]
    pallas_call x0 -> x8, Pallas kernels: none -> 6.39 us  [the longest x2 3.28 us: projected(): pl.pallas_call(functools.partial(up_kernel, layer, start, ny, nx, nz), ou...]
    dot_general x6 -> x0, matrix products: 5.86 us -> none  [the longest x2 3.09 us: body(): lax.dot_general(value_weight[layer], gained, TN, preferred_element_type=F32)]
    ppermute x0 -> x8, starting transfers between devices: none -> 4.85 us  [the longest x3 3.84 us: body(): piece = lax.ppermute(piece, 'y', [(i, (i + k) % ny) for i in range(ny)])]
  transfers between devices with their start and end apart: 4 -> 11, of which waited for: 4 -> 6; matrix products, arithmetic and copies ran while one was open for 0% -> 4% of each run, Pallas kernels for 0% -> 0%
where the time goes in v3:
time: 180 us; the launch traced here: 179 us
  blocking collectives  104 us (58%)
  waiting for transfers between devices  25.8 us (14%)
  starting transfers between devices  23.2 us (13%)
  local copies, waits for them, and re-layouts  17.8 us (10%)
  Pallas kernels  6.39 us (4%)
  other arithmetic  1.89 us (1%)
    all_to_all x5, blocking collectives, exchanged(): return lax.all_to_all(x, axis, split_axis=0, concat_axis=0, tiled=True)  104 us
    all_to_all x3, starting transfers between devices, exchanged(): return lax.all_to_all(x, axis, split_axis=0, concat_axis=0, tiled=True)  18.3 us
    all_to_all x3, waiting for transfers between devices, exchanged(): return lax.all_to_all(x, axis, split_axis=0, concat_axis=0, tiled=True)  14.3 us
    unnamed x38, local copies, waits for them, and re-layouts  13.9 us
    ppermute x3, waiting for transfers between devices, body(): piece = lax.ppermute(piece, 'y', [(i, (i + k) % ny) for i in range(ny)])  9.06 us
    ppermute x3, starting transfers between devices, body(): piece = lax.ppermute(piece, 'y', [(i, (i + k) % ny) for i in range(ny)])  3.84 us
  transfers between devices with their start and end apart: 11, of which 6 were waited for; matrix products, arithmetic and copies ran while one was open for 4% of the time, Pallas kernels for 0%

profile of v3, /device:TPU:2, one launch (start us, length us, event | category | flops | bytes accessed | tf_op | source)
XLA Modules:
  0.0 179.0 jit_solution(14809809099808520734)
XLA Ops:
  0.0 1.4 copy-done
  1.4 1.4 copy-done.1
  2.8 0.8 copy-done.11
  3.6 0.7 copy-done.12
  4.2 0.5 pack0.1
  4.7 18.1 %all_to_all.40.refs_0_ = bf16[4,912,128]{2,1,0:T(8,128)(2,1)S(1)} all-to-all(bf16[4,912,128]{2,1,0:T(8,128)(2,1)S(1)} %pack0.1), channel_id=1, replica_groups=mesh['z'=8,'y'=4,'x'=4,'dp'=2] {'y'}, dimensions={0} | all-to-all | bytes 1867776 | tf_op jit(solution)/shard_map/all_to_all | solution.py:24
  22.9 0.5 pack1.1
  23.3 2.0 %collective-permute-done.refs_1_ = bf16[4,912,128]{2,1,0:T(8,128)(2,1)S(1)} collective-permute-done((bf16[4,912,128]{2,1,0:T(8,128)(2,1)S(1)}, bf16[4,912,128]{2,1,0:T(8,128)(2,1)S(1)}, u32[]{:S(2)}, u32[]{:S(2)}) %collective-permute-start) | collective-permute-done | bytes 933920 | tf_op jit(solution)/shard_map/ppermute | solution.py:260
  25.4 1.5 up0.1
  26.8 8.6 %all-to-all-start.1 = ((bf16[8,208,128]{2,1,0:T(8,128)(2,1)}), bf16[8,208,128]{2,1,0:T(8,128)(2,1)S(1)}, u32[]{:S(2)}, u32[]{:S(2)}) async-start(bf16[8,208,128]{2,1,0:T(8,128)(2,1)} %up0.1), calls=%async_computation.1 | async-start | bytes 851968 | tf_op jit(solution)/shard_map/all_to_all | solution.py:24
  35.4 1.7 copy.31
  37.1 1.6 copy.32
  38.7 1.6 copy.33
  40.3 1.6 copy.34
  41.9 1.0 convert_bitcast_fusion
  43.0 0.6 collective-permute-start.1
  43.6 2.1 %collective-permute-start.2 = (bf16[768,128]{1,0:T(8,128)(2,1)S(1)}, bf16[768,128]{1,0:T(8,128)(2,1)}, u32[]{:S(2)}, u32[]{:S(2)}) collective-permute-start(bf16[768,128]{1,0:T(8,128)(2,1)S(1)} %get-tuple-element.24), channel_id=1, source_target_pairs={{0,16},{8,24},{16,0},{24,8},{1,17},{9,25},{17,1},{25,9},{2,18},{10... | collective-permute-start | bytes 589832 | tf_op jit(solution)/shard_map/ppermute | solution.py:267
  45.7 1.1 collective-permute-start.3
  46.8 8.3 %collective-permute-done.1.refs_3_ = bf16[768,128]{1,0:T(8,128)(2,1)S(1)} collective-permute-done((bf16[768,128]{1,0:T(8,128)(2,1)S(1)}, bf16[768,128]{1,0:T(8,128)(2,1)S(1)}, u32[]{:S(2)}, u32[]{:S(2)}) %collective-permute-start.1) | collective-permute-done | bytes 196640 | tf_op jit(solution)/shard_map/ppermute | solution.py:267
  55.2 0.7 collective-permute-done.3.refs_5_
  55.9 0.3 mid.2
  56.2 32.5 %all_to_all.41 = bf16[32,96,128]{2,1,0:T(8,128)(2,1)S(1)} all-to-all(bf16[32,96,128]{2,1,0:T(8,128)(2,1)S(1)} %mid.2), channel_id=1, replica_groups=mesh['z'=8,'y'=4,'x'=4,'dp'=2] {'y','z'}, dimensions={0} | all-to-all | bytes 1572864 | tf_op jit(solution)/shard_map/all_to_all | solution.py:24
  88.7 1.2 down0.1
  89.9 4.9 %all-to-all-start.3 = ((bf16[16,128,128]{2,1,0:T(8,128)(2,1)}), bf16[16,128,128]{2,1,0:T(8,128)(2,1)S(1)}, u32[]{:S(2)}, u32[]{:S(2)}) async-start(bf16[16,128,128]{2,1,0:T(8,128)(2,1)} %down0.1), calls=%async_computation.3 | async-start | bytes 1048576 | tf_op jit(solution)/shard_map/all_to_all | solution.py:24
  94.9 0.5 collective-permute-start.5
  95.4 0.1 collective-permute-start.6
  95.5 0.4 collective-permute-start.7
  95.9 0.4 collective-permute-done.4.refs_6_
  96.3 0.7 copy-done.3
  97.0 0.7 copy-done.5
  97.7 0.7 copy-done.7
  98.4 0.7 copy-done.9
  99.0 4.6 %all-to-all-done.3.refs_1_ = bf16[16,128,128]{2,1,0:T(8,128)(2,1)S(1)} async-done(((bf16[16,128,128]{2,1,0:T(8,128)(2,1)}), bf16[16,128,128]{2,1,0:T(8,128)(2,1)S(1)}, u32[]{:S(2)}, u32[]{:S(2)}) %all-to-all-start.3) | async-done | bytes 524320 | tf_op jit(solution)/shard_map/all_to_all | solution.py:24
  103.6 0.9 copy-done.4
  104.6 0.9 copy-done.6
  105.5 0.9 copy-done.8
  106.4 0.9 copy-done.10
  107.4 1.8 %up1.1 = (bf16[8,208,128]{2,1,0:T(8,128)(2,1)S(1)}, bf16[128,128]{1,0:T(8,128)(2,1)S(1)}) custom-call(bf16[4,912,128]{2,1,0:T(8,128)(2,1)S(1)} %all_to_all.40.refs_0_, bf16[16,128,128]{2,1,0:T(8,128)(2,1)S(1)} %all-to-all-done.3.refs_1_, bf16[768,128]{1,0:T(8,128)(2,1)S(1)} %get-tuple-element.17.refs_2_, ...), custom_call_target="tpu_custom_call" | custom-call | flops 201326592 | bytes 1572864 | tf_op jit(solution)/shard_map/up1/pallas_call | solution.py:164
  109.2 19.2 %all_to_all.42.parts = bf16[8,208,128]{2,1,0:T(8,128)(2,1)S(1)} all-to-all(bf16[8,208,128]{2,1,0:T(8,128)(2,1)S(1)} %get-tuple-element.22), channel_id=1, replica_groups=mesh['z'=8,'y'=4,'x'=4,'dp'=2] {'z'}, dimensions={0} | all-to-all | bytes 851968 | tf_op jit(solution)/shard_map/all_to_all | solution.py:24
  128.4 0.3 mid.3
  128.6 24.6 %all_to_all.43 = bf16[32,96,128]{2,1,0:T(8,128)(2,1)S(1)} all-to-all(bf16[32,96,128]{2,1,0:T(8,128)(2,1)S(1)} %mid.3), channel_id=1, replica_groups=mesh['z'=8,'y'=4,'x'=4,'dp'=2] {'y','z'}, dimensions={0} | all-to-all | bytes 1572864 | tf_op jit(solution)/shard_map/all_to_all | solution.py:24
  153.3 0.4 down1.1
  153.7 9.3 %all_to_all.44 = bf16[4,128,128]{2,1,0:T(8,128)(2,1)S(1)} all-to-all(bf16[4,128,128]{2,1,0:T(8,128)(2,1)S(1)} %down1.1), channel_id=1, replica_groups=mesh['z'=8,'y'=4,'x'=4,'dp'=2] {'x'}, dimensions={0} | all-to-all | bytes 262144 | tf_op jit(solution)/shard_map/all_to_all | solution.py:24
  163.0 0.1 fusion
  163.2 0.6 broadcast_in_dim.8
  163.8 4.8 %all-to-all-start.7 = ((bf16[32,2,128]{2,1,0:T(2,128)(2,1)}), bf16[32,2,128]{2,1,0:T(2,128)(2,1)S(1)}, u32[]{:S(2)}, u32[]{:S(2)}) async-start(bf16[32,2,128]{2,1,0:T(2,128)(2,1)} %broadcast_in_dim.8), calls=%async_computation.7 | async-start | bytes 32768 | tf_op jit(solution)/shard_map/all_to_all | solution.py:24
  168.6 9.7 %all-to-all-done.7 = bf16[32,2,128]{2,1,0:T(2,128)(2,1)S(1)} async-done(((bf16[32,2,128]{2,1,0:T(2,128)(2,1)}), bf16[32,2,128]{2,1,0:T(2,128)(2,1)S(1)}, u32[]{:S(2)}, u32[]{:S(2)}) %all-to-all-start.7) | async-done | bytes 16416 | tf_op jit(solution)/shard_map/all_to_all | solution.py:24
  178.3 0.7 fusion.2
  (40 shorter events, 0.2 us)
Async XLA Ops:
  0.0 1.4 copy-start
  1.4 1.4 copy-start.1
  2.8 0.8 copy-start.11
  3.6 0.7 copy-start.12
  22.9 2.5 %collective-permute-start = (bf16[4,912,128]{2,1,0:T(8,128)(2,1)S(1)}, bf16[4,912,128]{2,1,0:T(8,128)(2,1)S(1)}, u32[]{:S(2)}, u32[]{:S(2)}) collective-permute-start(bf16[4,912,128]{2,1,0:T(8,128)(2,1)S(1)} %all_to_all.40.refs_0_), channel_id=1, source_target_pairs={{0,1},{1,0},{2,3},{3,2},{4,5},{5,4},{6,7},{7,6},{8,9},{9,8},{10,11... | collective-permute-start | bytes 2801672 | tf_op jit(solution)/shard_map/ppermute | solution.py:260
  23.3 12.1 %copy-start.13 = (bf16[2,3,3072]{2,0,1:T(2,128)(2,1)S(1)}, bf16[2,3,3072]{2,0,1:T(2,128)(2,1)}, u32[]{:S(2)}) copy-start(bf16[2,3,3072]{2,0,1:T(2,128)(2,1)} %param.14) | copy-start | bytes 110596
  26.8 10.3 %copy-start.15 = (bf16[2,3072]{1,0:T(2,128)(2,1)S(1)}, bf16[2,3072]{1,0:T(2,128)(2,1)}, u32[]{:S(2)}) copy-start(bf16[2,3072]{1,0:T(2,128)(2,1)} %param.16) | copy-start | bytes 36868
  26.8 29.1 %all-to-all-start.1 = ((bf16[8,208,128]{2,1,0:T(8,128)(2,1)}), bf16[8,208,128]{2,1,0:T(8,128)(2,1)S(1)}, u32[]{:S(2)}, u32[]{:S(2)}) async-start(bf16[8,208,128]{2,1,0:T(8,128)(2,1)} %up0.1), calls=%async_computation.1 | async-start | bytes 851968 | tf_op jit(solution)/shard_map/all_to_all | solution.py:24
  35.4 3.3 %copy-start.14 = (bf16[2,3,3072]{2,0,1:T(2,128)(2,1)S(1)}, bf16[2,3,3072]{2,0,1:T(2,128)(2,1)}, u32[]{:S(2)}) copy-start(bf16[2,3,3072]{2,0,1:T(2,128)(2,1)} %param.15) | copy-start | bytes 110596
  37.1 3.2 %copy-start.16 = (bf16[2,3072]{1,0:T(2,128)(2,1)S(1)}, bf16[2,3072]{1,0:T(2,128)(2,1)}, u32[]{:S(2)}) copy-start(bf16[2,3072]{1,0:T(2,128)(2,1)} %param.17) | copy-start | bytes 36868
  43.0 45.8 %copy-start.2 = (bf16[2,3072,128]{2,1,0:T(8,128)(2,1)S(1)}, bf16[2,3072,128]{2,1,0:T(8,128)(2,1)}, u32[]{:S(2)}) copy-start(bf16[2,3072,128]{2,1,0:T(8,128)(2,1)} %weight.3) | copy-start | bytes 4718596
  43.0 12.2 %collective-permute-start.1 = (bf16[768,128]{1,0:T(8,128)(2,1)S(1)}, bf16[768,128]{1,0:T(8,128)(2,1)S(1)}, u32[]{:S(2)}, u32[]{:S(2)}) collective-permute-start(bf16[768,128]{1,0:T(8,128)(2,1)S(1)} %get-tuple-element.25), channel_id=1, source_target_pairs={{0,8},{8,16},{16,24},{24,0},{1,9},{9,17},{17,25},{25,1},{2,10},{10... | collective-permute-start | bytes 589832 | tf_op jit(solution)/shard_map/ppermute | solution.py:267
  43.6 11.5 %collective-permute-start.2 = (bf16[768,128]{1,0:T(8,128)(2,1)S(1)}, bf16[768,128]{1,0:T(8,128)(2,1)}, u32[]{:S(2)}, u32[]{:S(2)}) collective-permute-start(bf16[768,128]{1,0:T(8,128)(2,1)S(1)} %get-tuple-element.24), channel_id=1, source_target_pairs={{0,16},{8,24},{16,0},{24,8},{1,17},{9,25},{17,1},{25,9},{2,18},{10... | collective-permute-start | bytes 589832 | tf_op jit(solution)/shard_map/ppermute | solution.py:267
  45.7 10.2 %collective-permute-start.3 = (bf16[768,128]{1,0:T(8,128)(2,1)S(1)}, bf16[768,128]{1,0:T(8,128)(2,1)}, u32[]{:S(2)}, u32[]{:S(2)}) collective-permute-start(bf16[768,128]{1,0:T(8,128)(2,1)S(1)} %get-tuple-element.23), channel_id=1, source_target_pairs={{0,24},{8,0},{16,8},{24,16},{1,25},{9,1},{17,9},{25,17},{2,26},{10... | collective-permute-start | bytes 589832 | tf_op jit(solution)/shard_map/ppermute | solution.py:267
  89.9 13.7 %all-to-all-start.3 = ((bf16[16,128,128]{2,1,0:T(8,128)(2,1)}), bf16[16,128,128]{2,1,0:T(8,128)(2,1)S(1)}, u32[]{:S(2)}, u32[]{:S(2)}) async-start(bf16[16,128,128]{2,1,0:T(8,128)(2,1)} %down0.1), calls=%async_computation.3 | async-start | bytes 1048576 | tf_op jit(solution)/shard_map/all_to_all | solution.py:24
  94.9 1.4 collective-permute-start.4
  94.9 2.1 %collective-permute-start.5 = (bf16[768,128]{1,0:T(8,128)(2,1)S(1)}, bf16[768,128]{1,0:T(8,128)(2,1)S(1)}, u32[]{:S(2)}, u32[]{:S(2)}) collective-permute-start(bf16[768,128]{1,0:T(8,128)(2,1)S(1)} %collective-permute-done.1.refs_3_), channel_id=1, source_target_pairs={{0,1},{1,0},{2,3},{3,2},{4,5},{5,4},{6,7},{7,6},{8,9},{9,8},{10,11... | collective-permute-start | bytes 589832 | tf_op jit(solution)/shard_map/ppermute | solution.py:279
  95.4 2.3 %collective-permute-start.6 = (bf16[768,128]{1,0:T(8,128)(2,1)}, bf16[768,128]{1,0:T(8,128)(2,1)S(1)}, u32[]{:S(2)}, u32[]{:S(2)}) collective-permute-start(bf16[768,128]{1,0:T(8,128)(2,1)} %collective-permute-done.2.refs_4_), channel_id=1, source_target_pairs={{0,1},{1,0},{2,3},{3,2},{4,5},{5,4},{6,7},{7,6},{8,9},{9,8},{10,11... | collective-permute-start | bytes 589832 | tf_op jit(solution)/shard_map/ppermute | solution.py:279
  95.5 2.9 %collective-permute-start.7 = (bf16[768,128]{1,0:T(8,128)(2,1)}, bf16[768,128]{1,0:T(8,128)(2,1)S(1)}, u32[]{:S(2)}, u32[]{:S(2)}) collective-permute-start(bf16[768,128]{1,0:T(8,128)(2,1)} %collective-permute-done.3.refs_5_), channel_id=1, source_target_pairs={{0,1},{1,0},{2,3},{3,2},{4,5},{5,4},{6,7},{7,6},{8,9},{9,8},{10,11... | collective-permute-start | bytes 589832 | tf_op jit(solution)/shard_map/ppermute | solution.py:279
  96.3 0.7 copy-start.3
  97.0 0.7 copy-start.5
  97.7 0.7 copy-start.7
  98.4 0.7 copy-start.9
  103.6 0.9 copy-start.4
  104.6 0.9 copy-start.6
  105.5 0.9 copy-start.8
  106.4 0.9 copy-start.10
  153.2 15.3 %copy-start.17 = (bf16[128]{0:T(256)(128)(2,1)S(1)}, bf16[128]{0:T(256)(128)(2,1)}, u32[]{:S(2)}) copy-start(bf16[128]{0:T(256)(128)(2,1)} %param.19) | copy-start | bytes 772
  163.8 14.5 %all-to-all-start.7 = ((bf16[32,2,128]{2,1,0:T(2,128)(2,1)}), bf16[32,2,128]{2,1,0:T(2,128)(2,1)S(1)}, u32[]{:S(2)}, u32[]{:S(2)}) async-start(bf16[32,2,128]{2,1,0:T(2,128)(2,1)} %broadcast_in_dim.8), calls=%async_computation.7 | async-start | bytes 32768 | tf_op jit(solution)/shard_map/all_to_all | solution.py:24

commit v4 on v3

v4 whole, which is shorter than its diff:
```python
import functools

import jax
import jax.numpy as jnp
from jax import lax
from jax.experimental import pallas as pl
from jax.experimental.pallas import tpu as pltpu
from jax.sharding import Mesh
from jax.sharding import PartitionSpec as P

D = 4096
LAYERS = 2
LANES = 128
EXTRA = 16
WHOLE_VMEM = 67043328
EPS = 1e-06
F32 = jnp.float32
BF16 = jnp.bfloat16
VMEM = pl.BlockSpec(memory_space=pltpu.VMEM)
HBM = pl.BlockSpec(memory_space=pltpu.MemorySpace.HBM)


def exchanged(x, axis):
    return lax.all_to_all(x, axis, split_axis=0, concat_axis=0, tiled=True)


def room(mebibytes):
    return pltpu.CompilerParams(vmem_limit_bytes=mebibytes * 1024 * 1024)


def cost(flops, moved):
    return pl.CostEstimate(flops=flops, bytes_accessed=moved, transcendentals=0)


def half_copies(up, down, layer, ny, core, at, out, start, sems, first):
    width, columns = up.shape[1:]
    each = columns // ny // LANES
    half = columns // ny // 2
    for j in range(each):
        low = pl.multiple_of((at * each + j) * LANES, LANES)
        yield pltpu.make_async_copy(
            up.at[layer, :, pl.ds(low, LANES)],
            out.at[pl.ds(start + j * width, width), :],
            sems.at[first + j],
        )
    low = pl.multiple_of((at * 2 + core) * half, half)
    yield pltpu.make_async_copy(
        down.at[layer, pl.ds(low, half), :],
        out.at[pl.ds(start + each * width, half), :],
        sems.at[first + each],
    )


def pack_first_kernel(ny, gate, value, down, stream, gain, out, held, sems, more):
    tokens, width = stream.shape
    each = gate.shape[2] // ny // LANES + 1
    start = tokens + LAYERS * 8
    core = lax.axis_index("dp")
    others = [
        pltpu.make_async_copy(stream, out.at[i, pl.ds(0, tokens), :], more.at[i]) for i in range(ny)
    ]
    others.append(pltpu.make_async_copy(gain, held, more.at[ny]))

    def copies(up):
        for i in range(ny):
            yield from half_copies(up, down, 0, ny, core, i, out.at[i], start, sems, i * each)

    @pl.when(core == 0)
    def _():
        for c in copies(gate):
            c.start()

    @pl.when(core == 1)
    def _():
        for c in copies(value):
            c.start()

    for c in others:
        c.start()
    others[-1].wait()
    gains = jnp.broadcast_to(held[...].astype(F32)[:, None, :], (LAYERS, 8, width))
    gains = gains.reshape(LAYERS * 8, width).astype(BF16)
    for i in range(ny):
        out[i, tokens : tokens + LAYERS * 8, :] = gains
    for c in others[:-1]:
        c.wait()
    for c in copies(gate):
        c.wait()


def packed_first(ny, gate, value, down, stream, gain):
    rows = gate.shape[1] * gate.shape[2] // ny // LANES + down.shape[1] // ny // 2
    rows += stream.shape[0] + LAYERS * 8
    each = gate.shape[2] // ny // LANES + 1
    return pl.pallas_call(
        functools.partial(pack_first_kernel, ny),
        out_shape=jax.ShapeDtypeStruct((ny, rows, LANES), BF16),
        in_specs=[HBM] * 5,
        out_specs=VMEM,
        scratch_shapes=[
            pltpu.VMEM(gain.shape, BF16),
            pltpu.SemaphoreType.DMA((ny * each,)),
            pltpu.SemaphoreType.DMA((ny + 1,)),
        ],
        cost_estimate=cost(1000000, 2 * ny * rows * LANES),
        compiler_params=pltpu.CompilerParams(
            vmem_limit_bytes=WHOLE_VMEM - 2 * ny * rows * LANES - 16384
        ),
        name="pack0",
    )(gate, value, down, stream, gain)


def pack_second_kernel(ny, gate, value, down, *refs):
    outs, sems = refs[:-1], refs[-1]
    each = gate.shape[2] // ny // LANES + 1
    core = lax.axis_index("dp")
    y = lax.axis_index("y")

    def copies(up, spare):
        for k in range(ny):
            at = lax.rem(y + k, ny)
            yield from half_copies(up, down, 1, ny, core, at, outs[k], 0, sems, k * each)
        yield from half_copies(spare, down, 1, ny, 1 - core, y, outs[ny], 0, sems, ny * each)

    @pl.when(core == 0)
    def _():
        for c in copies(gate, value):
            c.start()

    @pl.when(core == 1)
    def _():
        for c in copies(value, gate):
            c.start()

    for c in copies(gate, value):
        c.wait()


def packed_second(ny, gate, value, down):
    rows = gate.shape[1] * gate.shape[2] // ny // LANES + down.shape[1] // ny // 2
    each = gate.shape[2] // ny // LANES + 1
    return pl.pallas_call(
        functools.partial(pack_second_kernel, ny),
        out_shape=[jax.ShapeDtypeStruct((rows, LANES), BF16)] * (ny + 1),
        in_specs=[HBM] * 3,
        out_specs=[VMEM] * (ny + 1),
        scratch_shapes=[pltpu.SemaphoreType.DMA(((ny + 1) * each,))],
        cost_estimate=cost(1000000, 2 * ny * rows * LANES),
        compiler_params=pltpu.CompilerParams(vmem_limit_bytes=WHOLE_VMEM - 1490000),
        name="pack1",
    )(gate, value, down)


def high_and_low(squares):
    tokens = squares.shape[0]
    total = jnp.broadcast_to(jnp.sum(squares, axis=1, keepdims=True), (tokens, LANES)).T[0:EXTRA]
    high = total.astype(BF16).astype(F32)
    index = lax.broadcasted_iota(jnp.int32, (EXTRA, tokens), 0)
    return jnp.where(index == 0, high, jnp.where(index == 1, total - high, 0.0)).astype(BF16)


def up_kernel(layer, start, ny, nz, block, *refs):
    mine = refs[0]
    if layer == 0:
        weights = [(mine.at[k], refs[1].at[k]) for k in range(ny)]
        (out,) = refs[2:]
    else:
        fresh = refs[1]
        weights = [(refs[2 + k], refs[2 + ny + k]) for k in range(ny)]
        out, kept = refs[2 + 2 * ny :]
    tokens = LANES
    width = LANES
    units = block // nz
    core = lax.axis_index("dp")
    y = lax.axis_index("y")
    squares = jnp.zeros((tokens, LANES), F32)
    gained = []
    for k in range(ny):
        at = k if layer == 0 else lax.rem(y - k + ny, ny)
        if layer:
            values = fresh[:, at].astype(F32).reshape(tokens, width)
            if k == 0:
                kept[...] = values.astype(BF16)
        else:
            values = mine[at, 0:tokens, :].astype(F32)
        gain = mine[at, tokens : tokens + 16, :].astype(F32)[8 * layer : 8 * layer + 1]
        squares = squares + values * values
        gained.append((values * gain).astype(BF16))
    gained = jnp.concatenate(gained, axis=1)
    for side in range(2):
        rows = pl.multiple_of((core if side == 0 else 1 - core) * units, 16)
        for j in range(block // LANES):
            weight = jnp.concatenate(
                [w[side][pl.ds(start + j * width, width), :] for w in weights], axis=0
            )
            result = jnp.dot(gained, weight, preferred_element_type=F32).T.astype(BF16)
            low = j * LANES
            while low < (j + 1) * LANES:
                slot = low // units
                high = min((j + 1) * LANES, (slot + 1) * units)
                out[slot, pl.ds(rows + (low - slot * units), high - low), :] = result[
                    low - j * LANES : high - j * LANES
                ]
                low = high
    both = high_and_low(squares)
    for i in range(nz):
        out[i, 2 * units : 2 * units + EXTRA, :] = both


def projected(layer, start, block, ny, nz, args):
    units = block // nz
    shapes = [jax.ShapeDtypeStruct((nz, 2 * units + EXTRA, LANES), BF16)]
    if layer:
        shapes.append(jax.ShapeDtypeStruct((LANES, LANES), BF16))
    return pl.pallas_call(
        functools.partial(up_kernel, layer, start, ny, nz, block),
        out_shape=shapes,
        in_specs=[VMEM] * len(args),
        out_specs=[VMEM] * len(shapes),
        cost_estimate=cost(4 * ny * LANES * LANES * block, 4 * ny * LANES * block),
        compiler_params=room(8),
        name=f"up{layer}",
    )(*args)


def mid_kernel(length, parts, table, out):
    count, rows, tokens = parts.shape
    units = out.shape[1]
    total = parts[0].astype(F32)
    for i in range(1, count):
        total = total + parts[i].astype(F32)
    mean = (total[2 * units : 2 * units + 1] + total[2 * units + 1 : 2 * units + 2]) / D
    scale = lax.rsqrt(mean + EPS)
    position = lax.rem(lax.broadcasted_iota(jnp.int32, (units, tokens), 1), length)
    spread = jnp.concatenate([table[...]] * (LANES // 8), axis=0)
    columns = spread.T[0:units]

    def mixed(low, at):
        x = (total[low : low + units] * scale).astype(BF16).astype(F32)
        one = jnp.where(position >= 1, pltpu.roll(x, 1, 1), 0.0)
        two = jnp.where(position >= 2, pltpu.roll(x, 2, 1), 0.0)
        return (
            columns[:, at + 3 : at + 4]
            + two * columns[:, at : at + 1]
            + one * columns[:, at + 1 : at + 2]
            + x * columns[:, at + 2 : at + 3]
        )

    hidden = (jax.nn.gelu(mixed(0, 0)) * mixed(units, 4)).astype(BF16)
    for i in range(out.shape[0]):
        out[i] = hidden


def gated(parts, table, units, length):
    return pl.pallas_call(
        functools.partial(mid_kernel, length),
        out_shape=jax.ShapeDtypeStruct((parts.shape[0], units, parts.shape[2]), BF16),
        in_specs=[VMEM] * 2,
        out_specs=VMEM,
        cost_estimate=cost(1000000, parts.size * 2),
        compiler_params=room(6),
        name="mid",
    )(parts, table)


def down_kernel(layer, start, half, ny, nx, hidden, *refs):
    out = refs[-1]
    if layer == 0:
        sides = [[ref.at[k] for k in range(ny)] for ref in refs[:2]]
    else:
        sides = [refs[0:ny], refs[ny : 2 * ny]]
    nz, units, tokens = hidden.shape
    core = lax.axis_index("dp")
    y = lax.axis_index("y")
    term = 0.0
    for side, weights in enumerate(sides):
        first = (core if side == 0 else 1 - core) * (nz // 2)
        rows = hidden[pl.ds(first, nz // 2)].reshape(half, tokens).T
        weight = jnp.concatenate([w[pl.ds(start, half), :] for w in weights], axis=1)
        term = term + jnp.dot(rows, weight, preferred_element_type=F32)
    for k in range(ny):
        piece = term[:, k * LANES : (k + 1) * LANES]
        if layer == 0:
            out[:, k] = piece.reshape(ny * nx, -1, LANES).astype(BF16)
        else:
            at = lax.rem(y - k + ny, ny)
            for i in range(nx):
                out[at * nx + i] = piece.astype(BF16)


def lowered(layer, start, half, ny, nx, args):
    tokens = args[0].shape[2]
    count = ny * nx
    shape = (count, ny, tokens // count, LANES) if layer == 0 else (count, tokens, LANES)
    return pl.pallas_call(
        functools.partial(down_kernel, layer, start, half, ny, nx),
        out_shape=jax.ShapeDtypeStruct(shape, BF16),
        in_specs=[VMEM] * len(args),
        out_specs=VMEM,
        cost_estimate=cost(4 * half * ny * LANES * tokens, 4 * half * ny * LANES),
        compiler_params=room(8),
        name=f"down{layer}",
    )(*args)


def add_kernel(terms, mine, out):
    count, ny, piece, width = terms.shape
    place = lax.axis_index("y") * (count // ny) + lax.axis_index("x")
    total = terms[0].astype(F32)
    for i in range(1, count):
        total = total + terms[i].astype(F32)
    rows = pl.multiple_of(place * piece, piece)
    own = mine[:, pl.ds(rows, piece), :].astype(F32)
    fresh = (0.5 * own + total).astype(BF16)
    for i in range(count):
        out[i] = fresh


def added(terms, mine):
    return pl.pallas_call(
        add_kernel,
        out_shape=jax.ShapeDtypeStruct(terms.shape, BF16),
        in_specs=[VMEM] * 2,
        out_specs=VMEM,
        cost_estimate=cost(1000000, terms.size * 4),
        compiler_params=room(4),
        name="add",
    )(terms, mine)


def last_kernel(terms, kept, last, out):
    total = terms[0].astype(F32)
    for i in range(1, terms.shape[0]):
        total = total + terms[i].astype(F32)
    fresh = (0.5 * kept[...].astype(F32) + total).astype(BF16)
    last[...] = fresh
    values = fresh.astype(F32)
    both = high_and_low(values * values)
    for i in range(out.shape[0]):
        out[i] = both


def finished(terms, kept, copies):
    return pl.pallas_call(
        last_kernel,
        out_shape=[
            jax.ShapeDtypeStruct(kept.shape, BF16),
            jax.ShapeDtypeStruct((copies, EXTRA, terms.shape[1]), BF16),
        ],
        in_specs=[VMEM] * 2,
        out_specs=[VMEM] * 2,
        cost_estimate=cost(1000000, terms.size * 4),
        compiler_params=room(4),
        name="last",
    )(terms, kept)


def norm_kernel(last, parts, gain, out):
    tokens = last.shape[0]
    total = parts[0].astype(F32)
    for i in range(1, parts.shape[0]):
        total = total + parts[i].astype(F32)
    scale = lax.rsqrt((total[0:1] + total[1:2]) / D + EPS)
    column = jnp.broadcast_to(scale, (LANES, tokens)).T
    values = last[...].astype(F32) * column * gain[...].astype(F32)
    out[...] = values.astype(BF16)


def normed(last, parts, gain):
    return pl.pallas_call(
        norm_kernel,
        out_shape=jax.ShapeDtypeStruct(last.shape, BF16),
        in_specs=[VMEM] * 3,
        out_specs=VMEM,
        cost_estimate=cost(1000000, last.size * 4),
        compiler_params=room(4),
        name="norm",
    )(last, parts, gain)


def body(
    stream,
    norm_gain,
    gate_weight,
    value_weight,
    gate_taps,
    value_taps,
    gate_bias,
    value_bias,
    down_weight,
    final_gain,
):
    batch_rows, length, width = stream.shape
    tokens = batch_rows * length
    ny, nx, nz = lax.axis_size("y"), lax.axis_size("x"), lax.axis_size("z")
    block = gate_weight.shape[2] // ny
    half = block // 2
    units = block // nz
    start = tokens + LAYERS * 8
    swap = [(0, 1), (1, 0)]
    own = stream.reshape(tokens, width)

    mine = exchanged(packed_first(ny, gate_weight, value_weight, down_weight, own, norm_gain), "y")
    other = lax.ppermute(mine, "dp", swap)
    later = packed_second(ny, gate_weight, value_weight, down_weight)
    *later, mine = lax.optimization_barrier((*later, mine))
    near = [later[0]]
    for k in range(1, ny):
        near.append(lax.ppermute(later[k], "y", [(i, (i + k) % ny) for i in range(ny)]))

    lower = lax.axis_index("y") * block + lax.axis_index("z") * units
    table = jnp.concatenate(
        [gate_taps, gate_bias[:, None], value_taps, value_bias[:, None]], axis=1
    )
    table = lax.dynamic_slice_in_dim(table, lower, units, 2).astype(F32)
    table = jnp.pad(table, ((0, 0), (0, 0), (0, LANES - units)))

    (parts,) = projected(0, start, block, ny, nz, [mine, other])
    hidden = exchanged(gated(exchanged(parts, "z"), table[0], units, length), "z")
    terms = lowered(0, start + block, half, ny, nx, [hidden, mine, other])
    terms = exchanged(terms, ("y", "x"))
    fresh = exchanged(added(terms, mine), ("y", "x"))
    far = [later[ny]] + [lax.ppermute(piece, "dp", swap) for piece in near[1:]]

    parts, kept = projected(1, 0, block, ny, nz, [mine, fresh, *near, *far])
    hidden = exchanged(gated(exchanged(parts, "z"), table[1], units, length), "z")
    terms = exchanged(lowered(1, block, half, ny, nx, [hidden, *near, *far]), ("y", "x"))
    last, squares = finished(terms, kept, nz * ny)
    squares = exchanged(squares, ("z", "y"))
    mixed = normed(last, squares, final_gain[None])
    return mixed.reshape(batch_rows, length, width)


def solution(mesh):
    split = Mesh(
        mesh.devices.reshape(8, 4, mesh.shape["cb"], mesh.shape["dp"]), ("z", "y", "x", "dp")
    )
    ra = ("z", "y")
    return jax.shard_map(
        body,
        mesh=split,
        in_specs=(
            P("dp", None, ra),
            P(None, ra),
            P(None, ra, "x"),
            P(None, ra, "x"),
            P(None, None, "x"),
            P(None, None, "x"),
            P(None, "x"),
            P(None, "x"),
            P(None, "x", ra),
            P(ra),
        ),
        out_specs=P("dp", None, ra),
        check_vma=False,
    )
```

time: 180 us -> 169 us (0.939)
  local copies, waits for them, and re-layouts: 17.8 us -> 0.13 us
  Pallas kernels: 6.39 us -> 16 us
  waiting for transfers between devices: 25.8 us -> 35.3 us
  blocking collectives: 104 us -> 95.6 us
  starting transfers between devices: 23.2 us -> 21.1 us
    unnamed x38 -> x20, local copies, waits for them, and re-layouts: 13.9 us -> 0.09 us
    pallas_call x6 -> x9, Pallas kernels: 5.87 us -> 14.7 us  [the longest x2 4.46 us: projected(): pl.pallas_call(functools.partial(up_kernel, layer, start, ny, nz, block),...]
    all_to_all x5 -> x6, blocking collectives: 104 us -> 95.6 us  [exchanged(): return lax.all_to_all(x, axis, split_axis=0, concat_axis=0, tiled=True)]
    all_to_all x3, waiting for transfers between devices: 14.3 us -> 22.3 us  [exchanged(): return lax.all_to_all(x, axis, split_axis=0, concat_axis=0, tiled=True)]
    ppermute x7 -> x6, waiting for transfers between devices: 9.49 us -> 12.8 us  [the longest x3 12.8 us: body(): lax.ppermute(later[k], 'y', [(i, (i + k) % ny) for i in range(ny)])]
    ppermute x7 -> x6, starting transfers between devices: 4.85 us -> 4.34 us  [the longest x3 3.83 us: body(): lax.ppermute(later[k], 'y', [(i, (i + k) % ny) for i in range(ny)])]
  transfers between devices with their start and end apart: 11 -> 10, of which waited for: 6 -> 5; matrix products, arithmetic and copies ran while one was open for 4% -> 0% of each run, Pallas kernels for 0% -> 3%
where the time goes in v4:
time: 169 us; the launch traced here: 168 us
  blocking collectives  95.6 us (57%)
  waiting for transfers between devices  35.3 us (21%)
  starting transfers between devices  21.1 us (12%)
  Pallas kernels  16 us (9%)
    all_to_all x6, blocking collectives, exchanged(): return lax.all_to_all(x, axis, split_axis=0, concat_axis=0, tiled=True)  95.6 us
    all_to_all x3, waiting for transfers between devices, exchanged(): return lax.all_to_all(x, axis, split_axis=0, concat_axis=0, tiled=True)  22.3 us
    all_to_all x3, starting transfers between devices, exchanged(): return lax.all_to_all(x, axis, split_axis=0, concat_axis=0, tiled=True)  16.7 us
    ppermute x3, waiting for transfers between devices, body(): lax.ppermute(later[k], 'y', [(i, (i + k) % ny) for i in range(ny)])  12.8 us
    pallas_call x2, Pallas kernels, projected(): pl.pallas_call(functools.partial(up_kernel, layer, start, ny, nz, block),...  4.46 us
    ppermute x3, starting transfers between devices, body(): lax.ppermute(later[k], 'y', [(i, (i + k) % ny) for i in range(ny)])  3.83 us
  transfers between devices with their start and end apart: 10, of which 5 were waited for; matrix products, arithmetic and copies ran while one was open for 0% of the time, Pallas kernels for 3%

profile of v4, /device:TPU:2, one launch (start us, length us, event | category | flops | bytes accessed | tf_op | source)
XLA Modules:
  0.0 168.4 jit_solution(4224410510741005257)
XLA Ops:
  0.0 2.7 %pack0.1 = bf16[4,1296,128]{2,1,0:T(8,128)(2,1)} custom-call(bf16[2,128,3072]{2,1,0:T(8,128)(2,1)} %gate.3, bf16[2,128,3072]{2,1,0:T(8,128)(2,1)} %value.3, bf16[2,3072,128]{2,1,0:T(8,128)(2,1)} %down.3, bf16[128,128]{1,0:T(8,128)(2,1)} %bitcast.10, bf16[2,128]{1,0:T(2,128)(2,1)} %gain.1), custom_call_target="tpu_custom_call" | custom-call | flops 1000000 | bytes 1327104 | tf_op jit(solution)/shard_map/pack0/pallas_call | solution.py:95
  2.7 22.6 %all_to_all.45.refs_0_.mine = bf16[4,1296,128]{2,1,0:T(8,128)(2,1)S(1)} all-to-all(bf16[4,1296,128]{2,1,0:T(8,128)(2,1)} %pack0.1), channel_id=1, replica_groups=mesh['z'=8,'y'=4,'x'=4,'dp'=2] {'y'}, dimensions={0} | all-to-all | bytes 2654208 | tf_op jit(solution)/shard_map/all_to_all | solution.py:24
  25.3 0.0 collective-permute-start
  25.3 2.9 %pack1.1 = (bf16[1152,128]{1,0:T(8,128)(2,1)}, bf16[1152,128]{1,0:T(8,128)(2,1)}, bf16[1152,128]{1,0:T(8,128)(2,1)}, bf16[1152,128]{1,0:T(8,128)(2,1)}, bf16[1152,128]{1,0:T(8,128)(2,1)}) custom-call(bf16[2,128,3072]{2,1,0:T(8,128)(2,1)} %gate.3, bf16[2,128,3072]{2,1,0:T(8,128)(2,1)} %value.3, bf16[2,3072,128]{2,1,0:T(8,128)(2,1)} %down.3), custom_call_target="tpu_custom_call" | custom-call | flops 1000000 | bytes 1179648 | tf_op jit(solution)/shard_map/pack1/pallas_call | solution.py:142
  28.2 0.0 copy-start.3
  28.2 0.0 copy-start.4
  28.2 0.0 copy-start.5
  28.2 0.0 copy-start.6
  28.3 0.2 collective-permute-done.refs_1_
  28.5 2.8 %up0.1 = bf16[8,208,128]{2,1,0:T(8,128)(2,1)} custom-call(bf16[4,1296,128]{2,1,0:T(8,128)(2,1)S(1)} %all_to_all.45.refs_0_.mine, bf16[4,1296,128]{2,1,0:T(8,128)(2,1)} %collective-permute-done.refs_1_), custom_call_target="tpu_custom_call" | custom-call | flops 201326592 | bytes 1572864 | tf_op jit(solution)/shard_map/up0/pallas_call | solution.py:215
  31.3 8.6 %all-to-all-start.1 = ((bf16[8,208,128]{2,1,0:T(8,128)(2,1)}), bf16[8,208,128]{2,1,0:T(8,128)(2,1)S(1)}, u32[]{:S(2)}, u32[]{:S(2)}) async-start(bf16[8,208,128]{2,1,0:T(8,128)(2,1)} %up0.1), calls=%async_computation.1 | async-start | bytes 851968 | tf_op jit(solution)/shard_map/all_to_all | solution.py:24
  39.9 0.0 copy-done.3
  39.9 0.0 copy-done.4
  39.9 0.0 copy-done.5
  40.0 0.0 copy-done.6
  40.0 0.1 fusion.2
  40.1 15.6 %all-to-all-done.1.parts = bf16[8,208,128]{2,1,0:T(8,128)(2,1)S(1)} async-done(((bf16[8,208,128]{2,1,0:T(8,128)(2,1)}), bf16[8,208,128]{2,1,0:T(8,128)(2,1)S(1)}, u32[]{:S(2)}, u32[]{:S(2)}) %all-to-all-start.1) | async-done | bytes 426016 | tf_op jit(solution)/shard_map/all_to_all | solution.py:24
  55.7 1.0 mid.2
  56.7 3.4 %all-to-all-start.2 = ((bf16[8,96,128]{2,1,0:T(8,128)(2,1)}), bf16[8,96,128]{2,1,0:T(8,128)(2,1)S(1)}, u32[]{:S(2)}, u32[]{:S(2)}) async-start(bf16[8,96,128]{2,1,0:T(8,128)(2,1)} %mid.2), calls=%async_computation.2 | async-start | bytes 393216 | tf_op jit(solution)/shard_map/all_to_all | solution.py:24
  60.1 0.6 collective-permute-start.1
  60.7 2.1 %collective-permute-start.2 = (bf16[1152,128]{1,0:T(8,128)(2,1)S(1)}, bf16[1152,128]{1,0:T(8,128)(2,1)S(1)}, u32[]{:S(2)}, u32[]{:S(2)}) collective-permute-start(bf16[1152,128]{1,0:T(8,128)(2,1)S(1)} %copy-done.7), channel_id=1, source_target_pairs={{0,16},{8,24},{16,0},{24,8},{1,17},{9,25},{17,1},{25,9},{2,18},{10... | collective-permute-start | bytes 884744 | tf_op jit(solution)/shard_map/ppermute | solution.py:409
  62.8 1.1 collective-permute-start.3
  63.9 12.7 %collective-permute-done.1.refs_3_.refs_1_ = bf16[1152,128]{1,0:T(8,128)(2,1)S(1)} collective-permute-done((bf16[1152,128]{1,0:T(8,128)(2,1)S(1)}, bf16[1152,128]{1,0:T(8,128)(2,1)S(1)}, u32[]{:S(2)}, u32[]{:S(2)}) %collective-permute-start.1) | collective-permute-done | bytes 294944 | tf_op jit(solution)/shard_map/ppermute | solution.py:409
  76.6 0.0 collective-permute-start.4
  76.6 0.0 collective-permute-done.2.refs_4_.refs_2_
  76.6 0.5 collective-permute-start.5
  77.1 0.1 collective-permute-done.3.refs_5_.refs_3_
  77.3 0.0 collective-permute-start.6
  77.3 0.0 all-to-all-done.2.hidden
  77.3 1.7 down0.1
  78.9 13.5 %all_to_all.46.terms = bf16[16,4,8,128]{3,2,1,0:T(8,128)(2,1)S(1)} all-to-all(bf16[16,4,8,128]{3,2,1,0:T(8,128)(2,1)S(1)} %down0.1), channel_id=1, replica_groups=mesh['z'=8,'y'=4,'x'=4,'dp'=2] {'y','x'}, dimensions={0} | all-to-all | bytes 262144 | tf_op jit(solution)/shard_map/all_to_all | solution.py:24
  92.4 0.7 add.11
  93.1 4.8 %all-to-all-start.4 = ((bf16[16,4,8,128]{3,2,1,0:T(8,128)(2,1)}), bf16[16,4,8,128]{3,2,1,0:T(8,128)(2,1)S(1)}, u32[]{:S(2)}, u32[]{:S(2)}) async-start(bf16[16,4,8,128]{3,2,1,0:T(8,128)(2,1)} %add.11), calls=%async_computation.4 | async-start | bytes 262144 | tf_op jit(solution)/shard_map/all_to_all | solution.py:24
  97.8 0.0 collective-permute-done.4.refs_7_.refs_5_
  97.8 0.0 collective-permute-done.5.refs_8_.refs_6_
  97.9 0.0 collective-permute-done.6.refs_9_.refs_7_
  97.9 6.7 %all-to-all-done.4.refs_1_ = bf16[16,4,8,128]{3,2,1,0:T(8,128)(2,1)S(1)} async-done(((bf16[16,4,8,128]{3,2,1,0:T(8,128)(2,1)}), bf16[16,4,8,128]{3,2,1,0:T(8,128)(2,1)S(1)}, u32[]{:S(2)}, u32[]{:S(2)}) %all-to-all-start.4) | async-done | bytes 131104 | tf_op jit(solution)/shard_map/all_to_all | solution.py:24
  104.6 0.0 copy-done.1
  104.6 1.7 up1.1
  106.2 20.3 %all_to_all.47.parts = bf16[8,208,128]{2,1,0:T(8,128)(2,1)S(1)} all-to-all(bf16[8,208,128]{2,1,0:T(8,128)(2,1)S(1)} %get-tuple-element.31), channel_id=1, replica_groups=mesh['z'=8,'y'=4,'x'=4,'dp'=2] {'z'}, dimensions={0} | all-to-all | bytes 851968 | tf_op jit(solution)/shard_map/all_to_all | solution.py:24
  126.5 0.3 mid.3
  126.8 12.2 %all_to_all.48.hidden = bf16[8,96,128]{2,1,0:T(8,128)(2,1)S(1)} all-to-all(bf16[8,96,128]{2,1,0:T(8,128)(2,1)S(1)} %mid.3), channel_id=1, replica_groups=mesh['z'=8,'y'=4,'x'=4,'dp'=2] {'z'}, dimensions={0} | all-to-all | bytes 393216 | tf_op jit(solution)/shard_map/all_to_all | solution.py:24
  139.0 1.3 down1.1
  140.3 0.0 copy-start.2
  140.3 13.5 %all_to_all.49.terms = bf16[16,128,128]{2,1,0:T(8,128)(2,1)S(1)} all-to-all(bf16[16,128,128]{2,1,0:T(8,128)(2,1)S(1)} %down1.1), channel_id=1, replica_groups=mesh['z'=8,'y'=4,'x'=4,'dp'=2] {'y','x'}, dimensions={0} | all-to-all | bytes 1048576 | tf_op jit(solution)/shard_map/all_to_all | solution.py:24
  153.9 0.2 last.1
  154.1 13.5 %all_to_all.50.parts = bf16[32,16,128]{2,1,0:T(8,128)(2,1)S(1)} all-to-all(bf16[32,16,128]{2,1,0:T(8,128)(2,1)S(1)} %get-tuple-element.34), channel_id=1, replica_groups=mesh['z'=8,'y'=4,'x'=4,'dp'=2] {'z','y'}, dimensions={0} | all-to-all | bytes 262144 | tf_op jit(solution)/shard_map/all_to_all | solution.py:24
  167.6 0.8 norm.1
  (14 shorter events, 0.1 us)
Async XLA Ops:
  25.3 3.2 %collective-permute-start = (bf16[4,1296,128]{2,1,0:T(8,128)(2,1)S(1)}, bf16[4,1296,128]{2,1,0:T(8,128)(2,1)}, u32[]{:S(2)}, u32[]{:S(2)}) collective-permute-start(bf16[4,1296,128]{2,1,0:T(8,128)(2,1)S(1)} %all_to_all.45.refs_0_.mine), channel_id=1, source_target_pairs={{0,1},{1,0},{2,3},{3,2},{4,5},{5,4},{6,7},{7,6},{8,9},{9,8},{10,11... | collective-permute-start | bytes 3981320 | tf_op jit(solution)/shard_map/ppermute | solution.py:404
  28.2 11.7 %copy-start.3 = (bf16[2,3,3072]{2,0,1:T(2,128)(2,1)S(1)}, bf16[2,3,3072]{2,0,1:T(2,128)(2,1)}, u32[]{:S(2)}) copy-start(bf16[2,3,3072]{2,0,1:T(2,128)(2,1)} %param.14) | copy-start | bytes 110596
  28.2 11.7 %copy-start.4 = (bf16[2,3,3072]{2,0,1:T(2,128)(2,1)S(1)}, bf16[2,3,3072]{2,0,1:T(2,128)(2,1)}, u32[]{:S(2)}) copy-start(bf16[2,3,3072]{2,0,1:T(2,128)(2,1)} %param.15) | copy-start | bytes 110596
  28.2 11.7 %copy-start.5 = (bf16[2,3072]{1,0:T(2,128)(2,1)S(1)}, bf16[2,3072]{1,0:T(2,128)(2,1)}, u32[]{:S(2)}) copy-start(bf16[2,3072]{1,0:T(2,128)(2,1)} %param.16) | copy-start | bytes 36868
  28.2 11.7 %copy-start.6 = (bf16[2,3072]{1,0:T(2,128)(2,1)S(1)}, bf16[2,3072]{1,0:T(2,128)(2,1)}, u32[]{:S(2)}) copy-start(bf16[2,3072]{1,0:T(2,128)(2,1)} %param.17) | copy-start | bytes 36868
  31.3 28.8 %copy-start.8 = (bf16[1152,128]{1,0:T(8,128)(2,1)S(1)}, bf16[1152,128]{1,0:T(8,128)(2,1)}, u32[]{:S(2)}) copy-start(bf16[1152,128]{1,0:T(8,128)(2,1)} %get-tuple-element.27) | copy-start | bytes 884740
  31.3 29.5 %copy-start.7 = (bf16[1152,128]{1,0:T(8,128)(2,1)S(1)}, bf16[1152,128]{1,0:T(8,128)(2,1)}, u32[]{:S(2)}) copy-start(bf16[1152,128]{1,0:T(8,128)(2,1)} %get-tuple-element.28) | copy-start | bytes 884740
  31.3 24.4 %all-to-all-start.1 = ((bf16[8,208,128]{2,1,0:T(8,128)(2,1)}), bf16[8,208,128]{2,1,0:T(8,128)(2,1)S(1)}, u32[]{:S(2)}, u32[]{:S(2)}) async-start(bf16[8,208,128]{2,1,0:T(8,128)(2,1)} %up0.1), calls=%async_computation.1 | async-start | bytes 851968 | tf_op jit(solution)/shard_map/all_to_all | solution.py:24
  56.7 20.6 %all-to-all-start.2 = ((bf16[8,96,128]{2,1,0:T(8,128)(2,1)}), bf16[8,96,128]{2,1,0:T(8,128)(2,1)S(1)}, u32[]{:S(2)}, u32[]{:S(2)}) async-start(bf16[8,96,128]{2,1,0:T(8,128)(2,1)} %mid.2), calls=%async_computation.2 | async-start | bytes 393216 | tf_op jit(solution)/shard_map/all_to_all | solution.py:24
  60.1 16.5 %collective-permute-start.1 = (bf16[1152,128]{1,0:T(8,128)(2,1)S(1)}, bf16[1152,128]{1,0:T(8,128)(2,1)S(1)}, u32[]{:S(2)}, u32[]{:S(2)}) collective-permute-start(bf16[1152,128]{1,0:T(8,128)(2,1)S(1)} %copy-done.8), channel_id=1, source_target_pairs={{0,8},{8,16},{16,24},{24,0},{1,9},{9,17},{17,25},{25,1},{2,10},{10... | collective-permute-start | bytes 884744 | tf_op jit(solution)/shard_map/ppermute | solution.py:409
  60.7 15.9 %collective-permute-start.2 = (bf16[1152,128]{1,0:T(8,128)(2,1)S(1)}, bf16[1152,128]{1,0:T(8,128)(2,1)S(1)}, u32[]{:S(2)}, u32[]{:S(2)}) collective-permute-start(bf16[1152,128]{1,0:T(8,128)(2,1)S(1)} %copy-done.7), channel_id=1, source_target_pairs={{0,16},{8,24},{16,0},{24,8},{1,17},{9,25},{17,1},{25,9},{2,18},{10... | collective-permute-start | bytes 884744 | tf_op jit(solution)/shard_map/ppermute | solution.py:409
  62.8 14.5 %collective-permute-start.3 = (bf16[1152,128]{1,0:T(8,128)(2,1)}, bf16[1152,128]{1,0:T(8,128)(2,1)S(1)}, u32[]{:S(2)}, u32[]{:S(2)}) collective-permute-start(bf16[1152,128]{1,0:T(8,128)(2,1)} %get-tuple-element.29), channel_id=1, source_target_pairs={{0,24},{8,0},{16,8},{24,16},{1,25},{9,1},{17,9},{25,17},{2,26},{10... | collective-permute-start | bytes 884744 | tf_op jit(solution)/shard_map/ppermute | solution.py:409
  76.6 21.2 %collective-permute-start.4 = (bf16[1152,128]{1,0:T(8,128)(2,1)S(1)}, bf16[1152,128]{1,0:T(8,128)(2,1)S(1)}, u32[]{:S(2)}, u32[]{:S(2)}) collective-permute-start(bf16[1152,128]{1,0:T(8,128)(2,1)S(1)} %collective-permute-done.1.refs_3_.refs_1_), channel_id=1, source_target_pairs={{0,1},{1,0},{2,3},{3,2},{4,5},{5,4},{6,7},{7,6},{8,9},{9,8},{10,11... | collective-permute-start | bytes 884744 | tf_op jit(solution)/shard_map/ppermute | solution.py:423
  76.6 21.2 %collective-permute-start.5 = (bf16[1152,128]{1,0:T(8,128)(2,1)S(1)}, bf16[1152,128]{1,0:T(8,128)(2,1)S(1)}, u32[]{:S(2)}, u32[]{:S(2)}) collective-permute-start(bf16[1152,128]{1,0:T(8,128)(2,1)S(1)} %collective-permute-done.2.refs_4_.refs_2_), channel_id=1, source_target_pairs={{0,1},{1,0},{2,3},{3,2},{4,5},{5,4},{6,7},{7,6},{8,9},{9,8},{10,11... | collective-permute-start | bytes 884744 | tf_op jit(solution)/shard_map/ppermute | solution.py:423
  77.3 20.6 %collective-permute-start.6 = (bf16[1152,128]{1,0:T(8,128)(2,1)S(1)}, bf16[1152,128]{1,0:T(8,128)(2,1)}, u32[]{:S(2)}, u32[]{:S(2)}) collective-permute-start(bf16[1152,128]{1,0:T(8,128)(2,1)S(1)} %collective-permute-done.3.refs_5_.refs_3_), channel_id=1, source_target_pairs={{0,1},{1,0},{2,3},{3,2},{4,5},{5,4},{6,7},{7,6},{8,9},{9,8},{10,11... | collective-permute-start | bytes 884744 | tf_op jit(solution)/shard_map/ppermute | solution.py:423
  78.9 25.6 %copy-start = (bf16[1152,128]{1,0:T(8,128)(2,1)S(1)}, bf16[1152,128]{1,0:T(8,128)(2,1)}, u32[]{:S(2)}) copy-start(bf16[1152,128]{1,0:T(8,128)(2,1)} %get-tuple-element.26.refs_2_.refs_0_) | copy-start | bytes 884740
  78.9 25.6 %copy-start.1 = (bf16[1152,128]{1,0:T(8,128)(2,1)S(1)}, bf16[1152,128]{1,0:T(8,128)(2,1)}, u32[]{:S(2)}) copy-start(bf16[1152,128]{1,0:T(8,128)(2,1)} %get-tuple-element.30.refs_6_.refs_4_) | copy-start | bytes 884740
  93.1 11.5 %all-to-all-start.4 = ((bf16[16,4,8,128]{3,2,1,0:T(8,128)(2,1)}), bf16[16,4,8,128]{3,2,1,0:T(8,128)(2,1)S(1)}, u32[]{:S(2)}, u32[]{:S(2)}) async-start(bf16[16,4,8,128]{3,2,1,0:T(8,128)(2,1)} %add.11), calls=%async_computation.4 | async-start | bytes 262144 | tf_op jit(solution)/shard_map/all_to_all | solution.py:24
  140.3 27.3 %copy-start.2 = (bf16[128]{0:T(256)(128)(2,1)S(1)}, bf16[128]{0:T(256)(128)(2,1)}, u32[]{:S(2)}) copy-start(bf16[128]{0:T(256)(128)(2,1)} %param.19) | copy-start | bytes 772

commit v5 on v4

--- a/solution.py
+++ b/solution.py
@@ -7,6 +7,7 @@
 from jax.experimental.pallas import tpu as pltpu
 from jax.sharding import Mesh
 from jax.sharding import PartitionSpec as P
+
 
 D = 4096
 LAYERS = 2
@@ -32,10 +33,9 @@
     return pl.CostEstimate(flops=flops, bytes_accessed=moved, transcendentals=0)
 
 
-def half_copies(up, down, layer, ny, core, at, out, start, sems, first):
+def up_copies(up, layer, ny, at, out, start, sems, first):
     width, columns = up.shape[1:]
     each = columns // ny // LANES
-    half = columns // ny // 2
     for j in range(each):
         low = pl.multiple_of((at * each + j) * LANES, LANES)
         yield pltpu.make_async_copy(
@@ -43,17 +43,22 @@
             out.at[pl.ds(start + j * width, width), :],
             sems.at[first + j],
         )
+
+
+def down_copies(down, ny, core, at, out, start, sems, first):
+    half = down.shape[1] // ny // 2
     low = pl.multiple_of((at * 2 + core) * half, half)
-    yield pltpu.make_async_copy(
-        down.at[layer, pl.ds(low, half), :],
-        out.at[pl.ds(start + each * width, half), :],
-        sems.at[first + each],
-    )
-
-
-def pack_first_kernel(ny, gate, value, down, stream, gain, out, held, sems, more):
+    for layer in range(LAYERS):
+        yield pltpu.make_async_copy(
+            down.at[layer, pl.ds(low, half), :],
+            out.at[pl.ds(start + layer * half, half), :],
+            sems.at[first + layer],
+        )
+
+
+def pack_first_kernel(ny, gate, value, stream, gain, out, held, sems, more):
     tokens, width = stream.shape
-    each = gate.shape[2] // ny // LANES + 1
+    each = gate.shape[2] // ny // LANES
     start = tokens + LAYERS * 8
     core = lax.axis_index("dp")
     others = [
@@ -63,7 +68,7 @@
 
     def copies(up):
         for i in range(ny):
-            yield from half_copies(up, down, 0, ny, core, i, out.at[i], start, sems, i * each)
+            yield from up_copies(up, 0, ny, i, out.at[i], start, sems, i * each)
 
     @pl.when(core == 0)
     def _():
@@ -88,14 +93,14 @@
         c.wait()
 
 
-def packed_first(ny, gate, value, down, stream, gain):
-    rows = gate.shape[1] * gate.shape[2] // ny // LANES + down.shape[1] // ny // 2
+def packed_first(ny, gate, value, stream, gain):
+    rows = gate.shape[1] * gate.shape[2] // ny // LANES
     rows += stream.shape[0] + LAYERS * 8
-    each = gate.shape[2] // ny // LANES + 1
+    each = gate.shape[2] // ny // LANES
     return pl.pallas_call(
         functools.partial(pack_first_kernel, ny),
         out_shape=jax.ShapeDtypeStruct((ny, rows, LANES), BF16),
-        in_specs=[HBM] * 5,
+        in_specs=[HBM] * 4,
         out_specs=VMEM,
         scratch_shapes=[
             pltpu.VMEM(gain.shape, BF16),
@@ -107,20 +112,24 @@
             vmem_limit_bytes=WHOLE_VMEM - 2 * ny * rows * LANES - 16384
         ),
         name="pack0",
-    )(gate, value, down, stream, gain)
+    )(gate, value, stream, gain)
 
 
 def pack_second_kernel(ny, gate, value, down, *refs):
     outs, sems = refs[:-1], refs[-1]
-    each = gate.shape[2] // ny // LANES + 1
+    ups = gate.shape[2] // ny // LANES
+    rows = ups * gate.shape[1]
+    each = ups + LAYERS
     core = lax.axis_index("dp")
     y = lax.axis_index("y")
 
     def copies(up, spare):
-        for k in range(ny):
-            at = lax.rem(y + k, ny)
-            yield from half_copies(up, down, 1, ny, core, at, outs[k], 0, sems, k * each)
-        yield from half_copies(spare, down, 1, ny, 1 - core, y, outs[ny], 0, sems, ny * each)
+        for k in range(ny + 1):
+            at = lax.rem(y + k, ny) if k < ny else y
+            side = core if k < ny else 1 - core
+            first = k * each
+            yield from up_copies(up if k < ny else spare, 1, ny, at, outs[k], 0, sems, first)
+            yield from down_copies(down, ny, side, at, outs[k], rows, sems, first + ups)
 
     @pl.when(core == 0)
     def _():
@@ -137,8 +146,8 @@
 
 
 def packed_second(ny, gate, value, down):
-    rows = gate.shape[1] * gate.shape[2] // ny // LANES + down.shape[1] // ny // 2
-    each = gate.shape[2] // ny // LANES + 1
+    rows = gate.shape[1] * gate.shape[2] // ny // LANES + LAYERS * down.shape[1] // ny // 2
+    each = gate.shape[2] // ny // LANES + LAYERS
     return pl.pallas_call(
         functools.partial(pack_second_kernel, ny),
         out_shape=[jax.ShapeDtypeStruct((rows, LANES), BF16)] * (ny + 1),
@@ -146,7 +155,7 @@
         out_specs=[VMEM] * (ny + 1),
         scratch_shapes=[pltpu.SemaphoreType.DMA(((ny + 1) * each,))],
         cost_estimate=cost(1000000, 2 * ny * rows * LANES),
-        compiler_params=pltpu.CompilerParams(vmem_limit_bytes=WHOLE_VMEM - 1490000),
+        compiler_params=room(4),
         name="pack1",
     )(gate, value, down)
 
@@ -219,12 +228,11 @@
         out_specs=[VMEM] * len(shapes),
         cost_estimate=cost(4 * ny * LANES * LANES * block, 4 * ny * LANES * block),
         compiler_params=room(8),
-        name=f"up{layer}",
     )(*args)
 
 
 def mid_kernel(length, parts, table, out):
-    count, rows, tokens = parts.shape
+    count, _, tokens = parts.shape
     units = out.shape[1]
     total = parts[0].astype(F32)
     for i in range(1, count):
@@ -265,11 +273,8 @@
 
 def down_kernel(layer, start, half, ny, nx, hidden, *refs):
     out = refs[-1]
-    if layer == 0:
-        sides = [[ref.at[k] for k in range(ny)] for ref in refs[:2]]
-    else:
-        sides = [refs[0:ny], refs[ny : 2 * ny]]
-    nz, units, tokens = hidden.shape
+    sides = [refs[0:ny], refs[ny : 2 * ny]]
+    nz, _, tokens = hidden.shape
     core = lax.axis_index("dp")
     y = lax.axis_index("y")
     term = 0.0
@@ -280,10 +285,10 @@
         term = term + jnp.dot(rows, weight, preferred_element_type=F32)
     for k in range(ny):
         piece = term[:, k * LANES : (k + 1) * LANES]
+        at = lax.rem(y - k + ny, ny)
         if layer == 0:
-            out[:, k] = piece.reshape(ny * nx, -1, LANES).astype(BF16)
+            out[:, at] = piece.reshape(ny * nx, -1, LANES).astype(BF16)
         else:
-            at = lax.rem(y - k + ny, ny)
             for i in range(nx):
                 out[at * nx + i] = piece.astype(BF16)
 
@@ -299,12 +304,11 @@
         out_specs=VMEM,
         cost_estimate=cost(4 * half * ny * LANES * tokens, 4 * half * ny * LANES),
         compiler_params=room(8),
-        name=f"down{layer}",
     )(*args)
 
 
 def add_kernel(terms, mine, out):
-    count, ny, piece, width = terms.shape
+    count, ny, piece, _ = terms.shape
     place = lax.axis_index("y") * (count // ny) + lax.axis_index("x")
     total = terms[0].astype(F32)
     for i in range(1, count):
@@ -378,7 +382,7 @@
     )(last, parts, gain)
 
 
-def body(
+def layers(
     stream,
     norm_gain,
     gate_weight,
@@ -400,10 +404,13 @@
     swap = [(0, 1), (1, 0)]
     own = stream.reshape(tokens, width)
 
-    mine = exchanged(packed_first(ny, gate_weight, value_weight, down_weight, own, norm_gain), "y")
+    mine = packed_first(ny, gate_weight, value_weight, own, norm_gain)
+    mine = exchanged(mine, "y")
     other = lax.ppermute(mine, "dp", swap)
+    (parts,) = projected(0, start, block, ny, nz, [mine, other])
+    parts = exchanged(parts, "z")
+
     later = packed_second(ny, gate_weight, value_weight, down_weight)
-    *later, mine = lax.optimization_barrier((*later, mine))
     near = [later[0]]
     for k in range(1, ny):
         near.append(lax.ppermute(later[k], "y", [(i, (i + k) % ny) for i in range(ny)]))
@@ -415,16 +422,17 @@
     table = lax.dynamic_slice_in_dim(table, lower, units, 2).astype(F32)
     table = jnp.pad(table, ((0, 0), (0, 0), (0, LANES - units)))
 
-    (parts,) = projected(0, start, block, ny, nz, [mine, other])
-    hidden = exchanged(gated(exchanged(parts, "z"), table[0], units, length), "z")
-    terms = lowered(0, start + block, half, ny, nx, [hidden, mine, other])
+    hidden = gated(parts, table[0], units, length)
+    hidden = exchanged(hidden, "z")
+    far = [later[ny]] + [lax.ppermute(piece, "dp", swap) for piece in near[1:]]
+    terms = lowered(0, block, half, ny, nx, [hidden, *near, *far])
     terms = exchanged(terms, ("y", "x"))
     fresh = exchanged(added(terms, mine), ("y", "x"))
-    far = [later[ny]] + [lax.ppermute(piece, "dp", swap) for piece in near[1:]]
 
     parts, kept = projected(1, 0, block, ny, nz, [mine, fresh, *near, *far])
     hidden = exchanged(gated(exchanged(parts, "z"), table[1], units, length), "z")
-    terms = exchanged(lowered(1, block, half, ny, nx, [hidden, *near, *far]), ("y", "x"))
+    terms = lowered(1, block + half, half, ny, nx, [hidden, *near, *far])
+    terms = exchanged(terms, ("y", "x"))
     last, squares = finished(terms, kept, nz * ny)
     squares = exchanged(squares, ("z", "y"))
     mixed = normed(last, squares, final_gain[None])
@@ -437,7 +445,7 @@
     )
     ra = ("z", "y")
     return jax.shard_map(
-        body,
+        layers,
         mesh=split,
         in_specs=(
             P("dp", None, ra),

time: 169 us -> 167 us (0.988)
  waiting for transfers between devices: 35.3 us -> 30.4 us
  local copies, waits for them, and re-layouts: 0.13 us -> 2.92 us
  blocking collectives: 95.6 us -> 97.4 us
    all_to_all x3 -> x2, waiting for transfers between devices: 22.3 us -> 11.1 us  [exchanged(): return lax.all_to_all(x, axis, split_axis=0, concat_axis=0, tiled=True)]
    ppermute x7, waiting for transfers between devices: 13.1 us -> 19.3 us  [the longest x3 16.8 us: layers(): lax.ppermute(later[k], 'y', [(i, (i + k) % ny) for i in range(ny)])]
    unnamed x20 -> x18, local copies, waits for them, and re-layouts: 0.09 us -> 2.88 us
    all_to_all x6 -> x7, blocking collectives: 95.6 us -> 97.4 us  [exchanged(): return lax.all_to_all(x, axis, split_axis=0, concat_axis=0, tiled=True)]
    all_to_all x3 -> x2, starting transfers between devices: 16.7 us -> 15.4 us  [exchanged(): return lax.all_to_all(x, axis, split_axis=0, concat_axis=0, tiled=True)]
  transfers between devices with their start and end apart: 10 -> 9, of which waited for: 5 -> 4; matrix products, arithmetic and copies ran while one was open for 0% -> 0% of each run, Pallas kernels for 3% -> 3%
where the time goes in v5:
time: 167 us; the launch traced here: 166 us
  blocking collectives  97.4 us (58%)
  waiting for transfers between devices  30.4 us (18%)
  starting transfers between devices  19.7 us (12%)
  Pallas kernels  15 us (9%)
  local copies, waits for them, and re-layouts  2.92 us (2%)
    all_to_all x7, blocking collectives, exchanged(): return lax.all_to_all(x, axis, split_axis=0, concat_axis=0, tiled=True)  97.4 us
    ppermute x3, waiting for transfers between devices, layers(): lax.ppermute(later[k], 'y', [(i, (i + k) % ny) for i in range(ny)])  16.8 us
    all_to_all x2, starting transfers between devices, exchanged(): return lax.all_to_all(x, axis, split_axis=0, concat_axis=0, tiled=True)  15.4 us
    all_to_all x2, waiting for transfers between devices, exchanged(): return lax.all_to_all(x, axis, split_axis=0, concat_axis=0, tiled=True)  11.1 us
    ppermute x3, starting transfers between devices, layers(): lax.ppermute(later[k], 'y', [(i, (i + k) % ny) for i in range(ny)])  3.84 us
  transfers between devices with their start and end apart: 9, of which 4 were waited for; matrix products, arithmetic and copies ran while one was open for 0% of the time, Pallas kernels for 3%

profile of v5, /device:TPU:2, one launch (start us, length us, event | category | flops | bytes accessed | tf_op | source)
XLA Modules:
  0.0 165.8 jit_solution(9892495169384477313)
XLA Ops:
  0.0 2.4 %pack0.1 = bf16[4,912,128]{2,1,0:T(8,128)(2,1)} custom-call(bf16[2,128,3072]{2,1,0:T(8,128)(2,1)} %gate.3, bf16[2,128,3072]{2,1,0:T(8,128)(2,1)} %value.3, bf16[128,128]{1,0:T(8,128)(2,1)} %bitcast.10, bf16[2,128]{1,0:T(2,128)(2,1)} %gain.1), custom_call_target="tpu_custom_call" | custom-call | flops 1000000 | bytes 933888 | tf_op jit(solution)/shard_map/pack0/pallas_call | solution.py:100
  2.4 18.4 %all_to_all.45.refs_0_.mine = bf16[4,912,128]{2,1,0:T(8,128)(2,1)S(1)} all-to-all(bf16[4,912,128]{2,1,0:T(8,128)(2,1)} %pack0.1), channel_id=1, replica_groups=mesh['z'=8,'y'=4,'x'=4,'dp'=2] {'y'}, dimensions={0} | all-to-all | bytes 1867776 | tf_op jit(solution)/shard_map/all_to_all | solution.py:25
  20.7 0.0 copy-start
  20.8 0.0 collective-permute-start
  20.8 2.5 %collective-permute-done.refs_1_ = bf16[4,912,128]{2,1,0:T(8,128)(2,1)S(1)} collective-permute-done((bf16[4,912,128]{2,1,0:T(8,128)(2,1)S(1)}, bf16[4,912,128]{2,1,0:T(8,128)(2,1)S(1)}, u32[]{:S(2)}, u32[]{:S(2)}) %collective-permute-start) | collective-permute-done | bytes 933920 | tf_op jit(solution)/shard_map/ppermute | solution.py:409
  23.2 1.4 shard_map.100
  24.7 8.5 %all-to-all-start.1 = ((bf16[8,208,128]{2,1,0:T(8,128)(2,1)}), bf16[8,208,128]{2,1,0:T(8,128)(2,1)}, u32[]{:S(2)}, u32[]{:S(2)}) async-start(bf16[8,208,128]{2,1,0:T(8,128)(2,1)} %shard_map.100), calls=%async_computation.1 | async-start | bytes 851968 | tf_op jit(solution)/shard_map/all_to_all | solution.py:25
  33.2 0.0 copy-done
  33.2 0.0 copy-start.1
  33.2 1.4 copy-done.1
  34.6 0.0 copy-start.2
  34.6 1.4 copy-done.2
  36.0 3.1 %pack1.1 = (bf16[1536,128]{1,0:T(8,128)(2,1)S(1)}, bf16[1536,128]{1,0:T(8,128)(2,1)}, bf16[1536,128]{1,0:T(8,128)(2,1)}, bf16[1536,128]{1,0:T(8,128)(2,1)}, bf16[1536,128]{1,0:T(8,128)(2,1)S(1)}) custom-call(bf16[2,128,3072]{2,1,0:T(8,128)(2,1)S(1)} %copy-done, bf16[2,128,3072]{2,1,0:T(8,128)(2,1)S(1)} %copy-done.1, bf16[2,3072,128]{2,1,0:T(8,128)(2,1)S(1)} %copy-done.2), custom_call_target="tpu_custom_call" | custom-call | flops 1000000 | bytes 1572864 | tf_op jit(solution)/shard_map/pack1/pallas_call | solution.py:151
  39.1 0.6 collective-permute-start.1
  39.8 2.1 %collective-permute-start.2 = (bf16[1536,128]{1,0:T(8,128)(2,1)}, bf16[1536,128]{1,0:T(8,128)(2,1)S(1)}, u32[]{:S(2)}, u32[]{:S(2)}) collective-permute-start(bf16[1536,128]{1,0:T(8,128)(2,1)} %get-tuple-element.16), channel_id=1, source_target_pairs={{0,16},{8,24},{16,0},{24,8},{1,17},{9,25},{17,1},{25,9},{2,18},{10... | collective-permute-start | bytes 1179656 | tf_op jit(solution)/shard_map/ppermute | solution.py:416
  41.9 1.1 collective-permute-start.3
  43.0 0.0 copy-done.6
  43.0 0.0 copy-done.7
  43.1 0.0 copy-done.4
  43.1 0.0 copy-done.5
  43.1 0.1 fusion.2
  43.2 16.7 %collective-permute-done.1.refs_1_.refs_3_ = bf16[1536,128]{1,0:T(8,128)(2,1)S(1)} collective-permute-done((bf16[1536,128]{1,0:T(8,128)(2,1)}, bf16[1536,128]{1,0:T(8,128)(2,1)S(1)}, u32[]{:S(2)}, u32[]{:S(2)}) %collective-permute-start.1) | collective-permute-done | bytes 393248 | tf_op jit(solution)/shard_map/ppermute | solution.py:416
  60.0 0.0 collective-permute-start.4
  60.0 0.0 collective-permute-done.2.refs_2_.refs_4_
  60.0 0.5 collective-permute-start.5
  60.5 0.1 collective-permute-done.3.refs_3_.refs_5_
  60.6 0.0 collective-permute-start.6
  60.6 0.0 all-to-all-done.1.parts
  60.6 2.0 %mid.2 = bf16[8,96,128]{2,1,0:T(8,128)(2,1)} custom-call(bf16[8,208,128]{2,1,0:T(8,128)(2,1)} %all-to-all-done.1.parts, f32[8,128]{1,0:T(8,128)S(1)} %get-tuple-element.24.table), custom_call_target="tpu_custom_call" | custom-call | flops 1000000 | bytes 425984 | tf_op jit(solution)/shard_map/mid/pallas_call | solution.py:263
  62.6 6.9 %all-to-all-start.2 = ((bf16[8,96,128]{2,1,0:T(8,128)(2,1)}), bf16[8,96,128]{2,1,0:T(8,128)(2,1)S(1)}, u32[]{:S(2)}, u32[]{:S(2)}) async-start(bf16[8,96,128]{2,1,0:T(8,128)(2,1)} %mid.2), calls=%async_computation.2 | async-start | bytes 393216 | tf_op jit(solution)/shard_map/all_to_all | solution.py:25
  69.5 0.0 collective-permute-done.4.refs_5_.refs_7_
  69.5 0.0 collective-permute-done.5.refs_6_.refs_8_
  69.5 0.0 collective-permute-done.6.refs_7_.refs_9_
  69.5 11.1 %all-to-all-done.2.hidden = bf16[8,96,128]{2,1,0:T(8,128)(2,1)S(1)} async-done(((bf16[8,96,128]{2,1,0:T(8,128)(2,1)}), bf16[8,96,128]{2,1,0:T(8,128)(2,1)S(1)}, u32[]{:S(2)}, u32[]{:S(2)}) %all-to-all-start.2) | async-done | bytes 196640 | tf_op jit(solution)/shard_map/all_to_all | solution.py:25
  80.7 1.4 shard_map.101
  82.1 13.3 %all_to_all.46.terms = bf16[16,4,8,128]{3,2,1,0:T(8,128)(2,1)S(1)} all-to-all(bf16[16,4,8,128]{3,2,1,0:T(8,128)(2,1)S(1)} %shard_map.101), channel_id=1, replica_groups=mesh['z'=8,'y'=4,'x'=4,'dp'=2] {'y','x'}, dimensions={0} | all-to-all | bytes 262144 | tf_op jit(solution)/shard_map/all_to_all | solution.py:25
  95.4 11.1 %all_to_all.47.refs_1_ = bf16[16,4,8,128]{3,2,1,0:T(8,128)(2,1)S(1)} all-to-all(bf16[16,4,8,128]{3,2,1,0:T(8,128)(2,1)S(1)} %add.11), channel_id=1, replica_groups=mesh['z'=8,'y'=4,'x'=4,'dp'=2] {'y','x'}, dimensions={0} | all-to-all | bytes 262144 | tf_op jit(solution)/shard_map/all_to_all | solution.py:25
  106.5 1.8 %shard_map.102 = (bf16[8,208,128]{2,1,0:T(8,128)(2,1)S(1)}, bf16[128,128]{1,0:T(8,128)(2,1)S(1)}) custom-call(bf16[4,912,128]{2,1,0:T(8,128)(2,1)S(1)} %all_to_all.45.refs_0_.mine, bf16[16,4,8,128]{3,2,1,0:T(8,128)(2,1)S(1)} %all_to_all.47.refs_1_, bf16[1536,128]{1,0:T(8,128)(2,1)S(1)} %get-tuple-element.14.refs_0_.refs_2_, ...), custom_call_target="tpu_custom_call" | custom-call | flops 201326592 | bytes 1572864 | tf_op jit(solution)/shard_map/pallas_call | solution.py:224
  108.3 15.5 %all_to_all.48.parts = bf16[8,208,128]{2,1,0:T(8,128)(2,1)S(1)} all-to-all(bf16[8,208,128]{2,1,0:T(8,128)(2,1)S(1)} %get-tuple-element.19), channel_id=1, replica_groups=mesh['z'=8,'y'=4,'x'=4,'dp'=2] {'z'}, dimensions={0} | all-to-all | bytes 851968 | tf_op jit(solution)/shard_map/all_to_all | solution.py:25
  123.9 0.3 mid.3
  124.2 12.2 %all_to_all.49.hidden = bf16[8,96,128]{2,1,0:T(8,128)(2,1)S(1)} all-to-all(bf16[8,96,128]{2,1,0:T(8,128)(2,1)S(1)} %mid.3), channel_id=1, replica_groups=mesh['z'=8,'y'=4,'x'=4,'dp'=2] {'z'}, dimensions={0} | all-to-all | bytes 393216 | tf_op jit(solution)/shard_map/all_to_all | solution.py:25
  136.3 1.5 shard_map.103
  137.8 0.0 copy-start.3
  137.8 13.5 %all_to_all.50.terms = bf16[16,128,128]{2,1,0:T(8,128)(2,1)S(1)} all-to-all(bf16[16,128,128]{2,1,0:T(8,128)(2,1)S(1)} %shard_map.103), channel_id=1, replica_groups=mesh['z'=8,'y'=4,'x'=4,'dp'=2] {'y','x'}, dimensions={0} | all-to-all | bytes 1048576 | tf_op jit(solution)/shard_map/all_to_all | solution.py:25
  151.3 0.2 last.1
  151.5 13.5 %all_to_all.51.parts = bf16[32,16,128]{2,1,0:T(8,128)(2,1)S(1)} all-to-all(bf16[32,16,128]{2,1,0:T(8,128)(2,1)S(1)} %get-tuple-element.22), channel_id=1, replica_groups=mesh['z'=8,'y'=4,'x'=4,'dp'=2] {'z','y'}, dimensions={0} | all-to-all | bytes 262144 | tf_op jit(solution)/shard_map/all_to_all | solution.py:25
  165.1 0.0 copy-done.3
  165.1 0.8 norm.1
  (11 shorter events, 0.1 us)
Async XLA Ops:
  20.7 12.4 %copy-start = (bf16[2,128,3072]{2,1,0:T(8,128)(2,1)S(1)}, bf16[2,128,3072]{2,1,0:T(8,128)(2,1)}, u32[]{:S(2)}) copy-start(bf16[2,128,3072]{2,1,0:T(8,128)(2,1)} %gate.3) | copy-start | bytes 4718596
  20.8 2.5 %collective-permute-start = (bf16[4,912,128]{2,1,0:T(8,128)(2,1)S(1)}, bf16[4,912,128]{2,1,0:T(8,128)(2,1)S(1)}, u32[]{:S(2)}, u32[]{:S(2)}) collective-permute-start(bf16[4,912,128]{2,1,0:T(8,128)(2,1)S(1)} %all_to_all.45.refs_0_.mine), channel_id=1, source_target_pairs={{0,1},{1,0},{2,3},{3,2},{4,5},{5,4},{6,7},{7,6},{8,9},{9,8},{10,11... | collective-permute-start | bytes 2801672 | tf_op jit(solution)/shard_map/ppermute | solution.py:409
  24.7 35.9 %all-to-all-start.1 = ((bf16[8,208,128]{2,1,0:T(8,128)(2,1)}), bf16[8,208,128]{2,1,0:T(8,128)(2,1)}, u32[]{:S(2)}, u32[]{:S(2)}) async-start(bf16[8,208,128]{2,1,0:T(8,128)(2,1)} %shard_map.100), calls=%async_computation.1 | async-start | bytes 851968 | tf_op jit(solution)/shard_map/all_to_all | solution.py:25
  33.2 1.4 copy-start.1
  34.6 1.4 copy-start.2
  36.0 7.0 %copy-start.6 = (bf16[2,3072]{1,0:T(2,128)(2,1)S(1)}, bf16[2,3072]{1,0:T(2,128)(2,1)}, u32[]{:S(2)}) copy-start(bf16[2,3072]{1,0:T(2,128)(2,1)} %param.16) | copy-start | bytes 36868
  36.0 7.0 %copy-start.7 = (bf16[2,3072]{1,0:T(2,128)(2,1)S(1)}, bf16[2,3072]{1,0:T(2,128)(2,1)}, u32[]{:S(2)}) copy-start(bf16[2,3072]{1,0:T(2,128)(2,1)} %param.17) | copy-start | bytes 36868
  36.0 7.1 %copy-start.4 = (bf16[2,3,3072]{2,0,1:T(2,128)(2,1)S(1)}, bf16[2,3,3072]{2,0,1:T(2,128)(2,1)}, u32[]{:S(2)}) copy-start(bf16[2,3,3072]{2,0,1:T(2,128)(2,1)} %param.14) | copy-start | bytes 110596
  36.0 7.1 %copy-start.5 = (bf16[2,3,3072]{2,0,1:T(2,128)(2,1)S(1)}, bf16[2,3,3072]{2,0,1:T(2,128)(2,1)}, u32[]{:S(2)}) copy-start(bf16[2,3,3072]{2,0,1:T(2,128)(2,1)} %param.15) | copy-start | bytes 110596
  39.1 20.8 %collective-permute-start.1 = (bf16[1536,128]{1,0:T(8,128)(2,1)}, bf16[1536,128]{1,0:T(8,128)(2,1)S(1)}, u32[]{:S(2)}, u32[]{:S(2)}) collective-permute-start(bf16[1536,128]{1,0:T(8,128)(2,1)} %get-tuple-element.15), channel_id=1, source_target_pairs={{0,8},{8,16},{16,24},{24,0},{1,9},{9,17},{17,25},{25,1},{2,10},{10... | collective-permute-start | bytes 1179656 | tf_op jit(solution)/shard_map/ppermute | solution.py:416
  39.8 20.2 %collective-permute-start.2 = (bf16[1536,128]{1,0:T(8,128)(2,1)}, bf16[1536,128]{1,0:T(8,128)(2,1)S(1)}, u32[]{:S(2)}, u32[]{:S(2)}) collective-permute-start(bf16[1536,128]{1,0:T(8,128)(2,1)} %get-tuple-element.16), channel_id=1, source_target_pairs={{0,16},{8,24},{16,0},{24,8},{1,17},{9,25},{17,1},{25,9},{2,18},{10... | collective-permute-start | bytes 1179656 | tf_op jit(solution)/shard_map/ppermute | solution.py:416
  41.9 18.7 %collective-permute-start.3 = (bf16[1536,128]{1,0:T(8,128)(2,1)}, bf16[1536,128]{1,0:T(8,128)(2,1)S(1)}, u32[]{:S(2)}, u32[]{:S(2)}) collective-permute-start(bf16[1536,128]{1,0:T(8,128)(2,1)} %get-tuple-element.17), channel_id=1, source_target_pairs={{0,24},{8,0},{16,8},{24,16},{1,25},{9,1},{17,9},{25,17},{2,26},{10... | collective-permute-start | bytes 1179656 | tf_op jit(solution)/shard_map/ppermute | solution.py:416
  60.0 9.6 %collective-permute-start.4 = (bf16[1536,128]{1,0:T(8,128)(2,1)S(1)}, bf16[1536,128]{1,0:T(8,128)(2,1)S(1)}, u32[]{:S(2)}, u32[]{:S(2)}) collective-permute-start(bf16[1536,128]{1,0:T(8,128)(2,1)S(1)} %collective-permute-done.1.refs_1_.refs_3_), channel_id=1, source_target_pairs={{0,1},{1,0},{2,3},{3,2},{4,5},{5,4},{6,7},{7,6},{8,9},{9,8},{10,11... | collective-permute-start | bytes 1179656 | tf_op jit(solution)/shard_map/ppermute | solution.py:427
  60.0 9.6 %collective-permute-start.5 = (bf16[1536,128]{1,0:T(8,128)(2,1)S(1)}, bf16[1536,128]{1,0:T(8,128)(2,1)}, u32[]{:S(2)}, u32[]{:S(2)}) collective-permute-start(bf16[1536,128]{1,0:T(8,128)(2,1)S(1)} %collective-permute-done.2.refs_2_.refs_4_), channel_id=1, source_target_pairs={{0,1},{1,0},{2,3},{3,2},{4,5},{5,4},{6,7},{7,6},{8,9},{9,8},{10,11... | collective-permute-start | bytes 1179656 | tf_op jit(solution)/shard_map/ppermute | solution.py:427
  60.6 9.0 %collective-permute-start.6 = (bf16[1536,128]{1,0:T(8,128)(2,1)S(1)}, bf16[1536,128]{1,0:T(8,128)(2,1)}, u32[]{:S(2)}, u32[]{:S(2)}) collective-permute-start(bf16[1536,128]{1,0:T(8,128)(2,1)S(1)} %collective-permute-done.3.refs_3_.refs_5_), channel_id=1, source_target_pairs={{0,1},{1,0},{2,3},{3,2},{4,5},{5,4},{6,7},{7,6},{8,9},{9,8},{10,11... | collective-permute-start | bytes 1179656 | tf_op jit(solution)/shard_map/ppermute | solution.py:427
  62.6 18.1 %all-to-all-start.2 = ((bf16[8,96,128]{2,1,0:T(8,128)(2,1)}), bf16[8,96,128]{2,1,0:T(8,128)(2,1)S(1)}, u32[]{:S(2)}, u32[]{:S(2)}) async-start(bf16[8,96,128]{2,1,0:T(8,128)(2,1)} %mid.2), calls=%async_computation.2 | async-start | bytes 393216 | tf_op jit(solution)/shard_map/all_to_all | solution.py:25
  137.8 27.3 %copy-start.3 = (bf16[128]{0:T(256)(128)(2,1)S(1)}, bf16[128]{0:T(256)(128)(2,1)}, u32[]{:S(2)}) copy-start(bf16[128]{0:T(256)(128)(2,1)} %param.19) | copy-start | bytes 772
